TPU v7x, 32 devices: a whole 2x2x4 slice. The times are simulated.
32 devices in a mesh: sp: 4 (over z), tp: 4 (over y, x), dp: 2 (over core).
Axes of the slice: x: 2, y: 2, z: 4, core: 2. Of those that a mesh axis runs over, the one named last changes fastest.
Arguments:
- latent: bfloat16 [2, 2048, 2048], P('dp', ('sp', 'tp')), may hold values from -6 to 6
- condition: float32 [2, 2048], P('dp'), may hold values from -6 to 6
- context: bfloat16 [2, 1024, 2048], P('dp', 'sp'), may hold values from -6 to 6
- context_cond: float32 [2048], replicated, may hold values from -6 to 6
- shift_matrix: bfloat16 [2048, 2048], P(('sp', 'tp')), may hold values from -0.125 to 0.125
- scale_matrix: bfloat16 [2048, 2048], P(('sp', 'tp')), may hold values from -0.125 to 0.125
- gate_matrix: bfloat16 [2048, 2048], P(('sp', 'tp')), may hold values from -0.125 to 0.125
- value_proj: bfloat16 [2048, 2048], P(None, 'tp'), may hold values from -0.125 to 0.125
- gate_proj: bfloat16 [2048, 2048], P(None, 'tp'), may hold values from -0.125 to 0.125
- write_proj: bfloat16 [2048, 1024], P(None, 'tp'), may hold values from -0.125 to 0.125
- read_proj: bfloat16 [2048, 1024], P(None, 'tp'), may hold values from -0.125 to 0.125
- step_proj: bfloat16 [2048, 2, 32], replicated, may hold values from -0.125 to 0.125
- decay_rate: float32 [2, 32], replicated, may hold values from 0.000243652344 to 0.0601
- pacing: float32 [2, 2048], P('dp'), may hold values from 0.2 to 4.3
- value_taps: float32 [5, 2048], replicated, may hold values from -2.5 to 2.5
- write_taps: float32 [5, 1024], replicated, may hold values from -2.5 to 2.5
- read_taps: float32 [5, 1024], replicated, may hold values from -2.5 to 2.5
- norm_gain: float32 [2048], replicated, may hold values from 0.1 to 1.9
- out_proj: bfloat16 [2048, 2048], P('tp'), may hold values from -0.125 to 0.125
Outputs:
- updated: bfloat16 [2, 2048, 2048], P('dp', ('sp', 'tp'))
All inputs are finite; a program needn't handle non-finite values.
Results may differ from a plain program's by a relative error of at most 0.006.
Values may be sent and summed in bfloat16 or wider, within the bound.
A program may use at most 128 MiB of HBM per device.

v0:
```python
import jax
import jax.numpy as jnp
from jax import lax
from jax.sharding import PartitionSpec as P

HEAD = 64
STATE = 128
ROW = 64
BLOCK = 128


NORM_FLOOR = 1e-05
GATED_FLOOR = 1e-06
FINEST = lax.Precision.HIGHEST


def masked_exp(exponent, allowed):
    return jnp.where(allowed, jnp.exp(jnp.where(allowed, exponent, 0.0)), 0.0)


def modulate(row_block, shift_row, scale_row):
    values = row_block.astype(jnp.float32)
    center = jnp.mean(values, -1, keepdims=True)
    spread = jnp.mean(jnp.square(values - center), -1, keepdims=True)
    normed = (values - center) * lax.rsqrt(spread + NORM_FLOOR)
    return (normed * (1.0 + shift_row * 0.0 + scale_row) + shift_row).astype(jnp.bfloat16)


def convolve(values, kernel, run_count):
    length, channels = values.shape
    tap_count = kernel.shape[0]
    margin = tap_count // 2
    stretch = length // run_count
    blocked = values.astype(jnp.float32).reshape(run_count, stretch, channels)
    padded = jnp.pad(blocked, ((0, 0), (margin, margin), (0, 0)))
    summed = jnp.zeros_like(blocked)
    for offset in range(tap_count):
        summed = summed + padded[:, offset : offset + stretch] * kernel[offset]
    return jax.nn.silu(summed).reshape(length, channels).astype(jnp.bfloat16)


def context_state(values, writes, weight, groups):
    length = values.shape[0]
    per_group = weight.shape[1] // groups
    scaled = (
        writes.reshape(length, groups, 1, STATE) * weight.reshape(length, groups, per_group, 1)
    ).astype(jnp.bfloat16)
    head_values = values.reshape(length, groups, per_group, HEAD)
    return jnp.einsum("lgrn,lgrp->grnp", scaled, head_values, preferred_element_type=jnp.float32)


def block_inputs(values, writes, decays, steps, groups):
    length = values.shape[0]
    per_group = decays.shape[1] // groups
    blocks = length // BLOCK
    head_values = values.reshape(blocks, BLOCK, groups, per_group, HEAD)
    write_rows = writes.reshape(blocks, BLOCK, groups, STATE)
    cumulative = jnp.cumsum(decays.reshape(blocks, BLOCK, groups, per_group), axis=1)
    step_rows = steps.reshape(blocks, BLOCK, groups, per_group)
    weight = jnp.exp(cumulative[:, -1:] - cumulative) * step_rows
    scaled = (write_rows[:, :, :, None, :] * weight[..., None]).astype(jnp.bfloat16)
    increment = jnp.einsum(
        "kqgrn,kqgrp->kgrnp", scaled, head_values, preferred_element_type=jnp.float32
    )

    def advance(carry_state, paired):
        block_decay, block_increment = paired
        return (jnp.exp(block_decay)[..., None, None] * carry_state + block_increment, carry_state)

    empty_state = jnp.zeros(increment.shape[1:], jnp.float32)
    final_state, before = lax.scan(advance, empty_state, (cumulative[:, -1], increment))
    return (cumulative, final_state, before)


def block_outputs(values, reads, affinity, cumulative, steps, before, start):
    blocks, block_rows, groups, per_group = cumulative.shape
    head_values = values.reshape(blocks, block_rows, groups, per_group, HEAD)
    read_rows = reads.reshape(blocks, block_rows, groups, STATE).astype(jnp.float32)
    step_rows = steps.reshape(blocks, block_rows, groups, per_group)
    lower_mask = jnp.tril(jnp.ones((block_rows, block_rows), bool))[:, :, None, None]
    exponent = cumulative[:, :, None] - cumulative[:, None, :]
    mixing = (affinity[..., None] * masked_exp(exponent, lower_mask) * step_rows[:, None]).astype(
        jnp.bfloat16
    )
    within = jnp.einsum(
        "ktsgr,ksgrp->ktgrp", mixing, head_values, preferred_element_type=jnp.float32
    )
    block_decay = cumulative[:, -1]
    earlier = jnp.cumsum(block_decay, axis=0) - block_decay
    entering = before + jnp.exp(earlier)[..., None, None] * start[None]
    carried = (
        jnp.einsum("ktgn,kgrnp->ktgrp", read_rows, entering, precision=FINEST)
        * jnp.exp(cumulative)[..., None]
    )
    return (within + carried).reshape(blocks * block_rows, groups * per_group * HEAD)


def per_device(
    latent,
    condition,
    context,
    context_cond,
    shift_matrix,
    scale_matrix,
    gate_matrix,
    value_proj,
    gate_proj,
    write_proj,
    read_proj,
    step_proj,
    decay_rate,
    pacing,
    value_taps,
    write_taps,
    read_taps,
    norm_gain,
    out_proj,
):
    sp_count = lax.axis_size("sp")
    sp_index = lax.axis_index("sp")
    tp_index = lax.axis_index("tp")
    model_width = latent.shape[2]
    width_dev = value_proj.shape[1]
    keys_dev = write_proj.shape[1]
    heads_dev = width_dev // HEAD
    groups_dev = keys_dev // STATE
    state_shape = (groups_dev, heads_dev // groups_dev, STATE, HEAD)
    row_share = shift_matrix.shape[0]
    activated = jax.nn.silu(jnp.stack([condition[0], context_cond])).astype(jnp.bfloat16)
    own_cols = lax.dynamic_slice_in_dim(
        activated, (sp_index * lax.axis_size("tp") + tp_index) * row_share, row_share, 1
    )
    shift_part = jnp.dot(own_cols, shift_matrix, preferred_element_type=jnp.float32)
    scale_part = jnp.dot(own_cols, scale_matrix, preferred_element_type=jnp.float32)
    gate_part = jnp.dot(own_cols[:1], gate_matrix, preferred_element_type=jnp.float32)
    shifts, scales, gate_row = lax.psum((shift_part, scale_part, gate_part), ("sp", "tp"))
    step_cols = lax.dynamic_slice_in_dim(step_proj, tp_index * heads_dev, heads_dev, 2).reshape(
        model_width, 2 * heads_dev
    )
    own_rows = modulate(latent[0], shifts[0], scales[0])
    row_piece = lax.all_gather(own_rows, "tp", axis=0, tiled=True)
    projected = jnp.concatenate(
        [
            jnp.dot(row_piece, value_proj, preferred_element_type=jnp.float32),
            jnp.dot(row_piece, gate_proj, preferred_element_type=jnp.float32),
            jnp.dot(row_piece, write_proj, preferred_element_type=jnp.float32),
            jnp.dot(row_piece, read_proj, preferred_element_type=jnp.float32),
            jnp.dot(row_piece, step_cols, preferred_element_type=jnp.float32),
        ],
        axis=1,
    )
    tokens = projected.shape[0]
    run_count = tokens // ROW
    gate_end = 2 * width_dev
    write_end = gate_end + keys_dev
    read_end = write_end + keys_dev
    value_kernel = lax.dynamic_slice_in_dim(value_taps, tp_index * width_dev, width_dev, 1)
    write_kernel = lax.dynamic_slice_in_dim(write_taps, tp_index * keys_dev, keys_dev, 1)
    read_kernel = lax.dynamic_slice_in_dim(read_taps, tp_index * keys_dev, keys_dev, 1)
    values = convolve(projected[:, :width_dev].astype(jnp.bfloat16), value_kernel, run_count)
    gate_pre = projected[:, width_dev:gate_end].astype(jnp.bfloat16)
    writes = convolve(
        projected[:, gate_end:write_end].astype(jnp.bfloat16), write_kernel, run_count
    )
    reads = convolve(projected[:, write_end:read_end].astype(jnp.bfloat16), read_kernel, run_count)
    step_raw = projected[:, read_end:].astype(jnp.bfloat16)
    latent_raw = (
        lax.optimization_barrier(step_raw).astype(jnp.float32).reshape(tokens, 2, heads_dev)
    )
    rates = lax.dynamic_slice_in_dim(decay_rate, tp_index * heads_dev, heads_dev, 1)
    local_pace = lax.dynamic_slice_in_dim(pacing[0], sp_index * tokens, tokens, 0)
    forward_step = jax.nn.softplus(latent_raw[:, 0]) * local_pace[:, None]
    forward_decay = -rates[0][None, :] * forward_step
    backward_step = jax.nn.softplus(latent_raw[:, 1]) * local_pace[:, None]
    backward_decay = -rates[1][None, :] * backward_step
    forward_cumul, forward_end, forward_before = block_inputs(
        values, writes, forward_decay, forward_step, groups_dev
    )
    backward_cumul, backward_end, backward_before = block_inputs(
        values[::-1], writes[::-1], backward_decay[::-1], backward_step[::-1], groups_dev
    )
    context_hidden = modulate(context[0], shifts[1], scales[1])
    context_value = jnp.dot(context_hidden, value_proj, preferred_element_type=jnp.float32).astype(
        jnp.bfloat16
    )
    context_write = jnp.dot(context_hidden, write_proj, preferred_element_type=jnp.float32).astype(
        jnp.bfloat16
    )
    context_raw = jnp.dot(context_hidden, step_cols, preferred_element_type=jnp.float32).astype(
        jnp.bfloat16
    )
    ctx_value_all, ctx_write_all, ctx_raw_all, latent_raw_all = (
        lax.all_gather(context_value, "sp", axis=0, tiled=True),
        lax.all_gather(context_write, "sp", axis=0, tiled=True),
        lax.all_gather(context_raw, "sp", axis=0, tiled=True),
        lax.all_gather(step_raw, "sp", axis=0, tiled=True),
    )
    ctx_values = convolve(ctx_value_all, value_kernel, 1)
    ctx_writes = convolve(ctx_write_all, write_kernel, 1)
    ctx_raw = lax.optimization_barrier(ctx_raw_all).astype(jnp.float32).reshape(-1, 2, heads_dev)
    ctx_fwd_step = jax.nn.softplus(ctx_raw[:, 0])
    ctx_fwd_decay = -rates[0][None, :] * ctx_fwd_step
    ctx_cumul = jnp.cumsum(ctx_fwd_decay, axis=0)
    ctx_forward = context_state(
        ctx_values, ctx_writes, jnp.exp(ctx_cumul[-1:] - ctx_cumul) * ctx_fwd_step, groups_dev
    )
    ctx_bwd_step = jax.nn.softplus(ctx_raw[:, 1])
    ctx_bwd_decay = -rates[1][None, :] * ctx_bwd_step
    ctx_back_cumul = jnp.cumsum(ctx_bwd_decay, axis=0)
    ctx_backward = context_state(
        ctx_values, ctx_writes, jnp.exp(ctx_back_cumul - ctx_bwd_decay) * ctx_bwd_step, groups_dev
    )
    ctx_forward = ctx_forward.reshape(heads_dev, STATE, HEAD)
    ctx_backward = ctx_backward.reshape(heads_dev, STATE, HEAD)
    empty_state = jnp.zeros((heads_dev, STATE, HEAD), jnp.float32)
    all_raw = (
        lax.optimization_barrier(latent_raw_all)
        .astype(jnp.float32)
        .reshape(sp_count, tokens, 2, heads_dev)
    )
    all_steps = jax.nn.softplus(all_raw) * pacing[0].reshape(sp_count, tokens)[:, :, None, None]
    totals = jnp.sum(-rates[None, None] * all_steps, axis=1)
    forward_totals = totals[:, 0]
    backward_totals = totals[:, 1]
    forward_prefix = jnp.cumsum(forward_totals, axis=0) - forward_totals
    backward_suffix = jnp.cumsum(backward_totals[::-1], axis=0)[::-1] - backward_totals
    forward_through = forward_prefix + forward_totals
    backward_through = backward_suffix + backward_totals
    own_prefix = forward_prefix[sp_index]
    own_suffix = backward_suffix[sp_index]
    forward_piece = lax.all_gather(
        forward_end.reshape(1, heads_dev, STATE, HEAD).astype(jnp.bfloat16),
        "sp",
        axis=0,
        tiled=True,
    ).astype(jnp.float32)
    backward_piece = lax.all_gather(
        backward_end.reshape(1, heads_dev, STATE, HEAD).astype(jnp.bfloat16),
        "sp",
        axis=0,
        tiled=True,
    ).astype(jnp.float32)
    shard_count = forward_piece.shape[0]
    sources = jnp.arange(shard_count)
    forward_gap = own_prefix[None] - forward_through
    backward_gap = own_suffix[None] - backward_through
    forward_weight = masked_exp(forward_gap, (sources < sp_index)[:, None])
    backward_weight = masked_exp(backward_gap, (sources > sp_index)[:, None])
    forward_in = empty_state + jnp.sum(forward_weight[:, :, None, None] * forward_piece, axis=0)
    backward_in = empty_state + jnp.sum(backward_weight[:, :, None, None] * backward_piece, axis=0)
    forward_start = forward_in + jnp.exp(own_prefix)[:, None, None] * ctx_forward
    backward_start = backward_in + jnp.exp(own_suffix)[:, None, None] * ctx_backward
    blocks = tokens // BLOCK
    forward_affinity = jnp.einsum(
        "ktgn,ksgn->ktsg",
        reads.reshape(blocks, BLOCK, groups_dev, STATE),
        writes.reshape(blocks, BLOCK, groups_dev, STATE),
        preferred_element_type=jnp.float32,
    )
    backward_affinity = forward_affinity[::-1, ::-1, ::-1]
    forward_out = block_outputs(
        values,
        reads,
        forward_affinity,
        forward_cumul,
        forward_step,
        forward_before,
        forward_start.reshape(state_shape),
    )
    backward_out = block_outputs(
        values[::-1],
        reads[::-1],
        backward_affinity,
        backward_cumul,
        backward_step[::-1],
        backward_before,
        backward_start.reshape(state_shape),
    )[::-1]
    gated_heads = (forward_out + backward_out) * jax.nn.silu(gate_pre.astype(jnp.float32))
    grouped = gated_heads.reshape(tokens, groups_dev, -1)
    grouped = grouped * lax.rsqrt(jnp.mean(grouped * grouped, -1, keepdims=True) + GATED_FLOOR)
    gain_dev = lax.dynamic_slice_in_dim(norm_gain, tp_index * width_dev, width_dev, 0)
    inner_rows = (grouped.reshape(tokens, width_dev) * gain_dev).astype(jnp.bfloat16)
    mixed = lax.psum_scatter(
        jnp.dot(inner_rows, out_proj, preferred_element_type=jnp.float32).astype(jnp.bfloat16),
        "tp",
        scatter_dimension=0,
        tiled=True,
    )
    updated = (
        latent[0].astype(jnp.float32)
        + gate_row[0] * lax.optimization_barrier(mixed).astype(jnp.float32)
    ).astype(jnp.bfloat16)
    return updated[None]


def solution(mesh):
    placed = (
        P("dp", ("sp", "tp"), None),
        P("dp", None),
        P("dp", "sp", None),
        P(),
        P(("sp", "tp"), None),
        P(("sp", "tp"), None),
        P(("sp", "tp"), None),
        P(None, "tp"),
        P(None, "tp"),
        P(None, "tp"),
        P(None, "tp"),
        P(),
        P(),
        P("dp", None),
        P(),
        P(),
        P(),
        P(),
        P("tp", None),
    )
    return jax.shard_map(
        per_device,
        mesh=mesh,
        in_specs=placed,
        out_specs=P("dp", ("sp", "tp"), None),
        check_vma=False,
    )
```

profile of v0, /device:TPU:0, one launch (start us, length us, event | category | flops | bytes accessed | tf_op | source)
XLA Modules:
  0.0 397.5 jit_solution(12184794722132868650)
XLA Ops:
  7.4 1.3 fusion.167
  11.9 79.3 %all-reduce.5 = (f32[2,2048]{1,0:T(2,128)S(1)}, f32[2,2048]{1,0:T(2,128)S(1)}, f32[2048]{0:T(1024)}) all-reduce(f32[2,2048]{1,0:T(2,128)S(1)} %fusion.167, f32[2,2048]{1,0:T(2,128)S(1)} %fusion.168, f32[2048]{0:T(1024)S(1)} %bitcast.335), channel_id=1, replica_groups=mesh['sp'=4,'tp'=4,'dp'=2] {'sp','tp'}, use_global_device_ids=true, to_apply=%region_3.4 | all-reduce | flops 10240 | bytes 81920 | tf_op jit(solution)/shard_map/psum | solution.py:136
  91.2 3.4 convolution_convert_fusion.3
  99.0 1.8 convolution_convert_fusion.8
  100.8 13.4 %all_gather.25 = bf16[1024,16]{0,1:T(8,128)(2,1)S(1)} all-gather(bf16[256,16]{0,1:T(8,128)(2,1)S(1)} %convolution_convert_fusion.8), channel_id=1, replica_groups=mesh['sp'=4,'tp'=4,'dp'=2] {'sp'}, dimensions={0}, use_global_device_ids=true | all-gather | bytes 40960 | tf_op jit(solution)/shard_map/all_gather | solution.py:195
  114.3 2.3 reduce-window.16
  116.8 2.3 reduce-window.14
  121.6 2.1 convolution_convert_fusion.6
  123.7 14.7 %all_gather.24 = bf16[1024,256]{1,0:T(8,128)(2,1)S(1)} all-gather(bf16[256,256]{1,0:T(8,128)(2,1)S(1)} %convolution_convert_fusion.6), channel_id=1, replica_groups=mesh['sp'=4,'tp'=4,'dp'=2] {'sp'}, dimensions={0}, use_global_device_ids=true | all-gather | bytes 655360 | tf_op jit(solution)/shard_map/all_gather | solution.py:194
  138.6 1.8 fusion.123
  140.3 2.8 reshape.548
  143.1 2.3 copy.191
  146.1 1.4 dynamic_slice.53
  150.1 1.6 convert_bitcast_fusion.1
  151.7 2.6 multiply_convert_fusion.6
  154.4 2.3 copy.193
  156.6 2.9 all-gather.3.cloned.1.call-done
  159.5 2.2 convolution_convert_fusion.7
  163.2 2.1 fusion.166
  165.2 1.8 copy.202
  167.8 14.1 %all_gather.22 = bf16[2048,16]{0,1:T(8,128)(2,1)} all-gather(bf16[512,16]{0,1:T(8,128)(2,1)S(1)} %convolution_convert_fusion.7), channel_id=1, replica_groups=mesh['sp'=4,'tp'=4,'dp'=2] {'sp'}, dimensions={0}, use_global_device_ids=true | all-gather | bytes 81920 | tf_op jit(solution)/shard_map/all_gather | solution.py:196
  181.9 1.4 fusion.53
  183.3 2.6 convolution_convert_fusion.4
  188.1 2.6 convolution_convert_fusion.5
  191.8 1.7 convert_element_type.233
  193.5 2.0 convolution_bitcast_fusion.2
  195.6 5.0 %rev.30 = f32[4,128,128,2]{1,2,3,0:T(8,128)} reverse(f32[4,128,128,2]{1,2,3,0:T(8,128)} %convolution_bitcast_fusion.2), dimensions={0,1,2} | reverse | bytes 1048576 | tf_op jit(solution)/shard_map/rev | solution.py:260
  200.6 2.0 copy.179
  203.7 2.1 fusion.165
  205.8 1.8 copy.181
  207.6 1.3 slice_bitcast_fusion.4
  208.9 1.8 copy.184
  210.7 1.4 fusion.54
  212.1 2.1 exp.175
  214.3 3.5 convolution_convert_fusion.2
  217.9 1.6 multiply_convert_fusion.22
  219.4 2.9 reshape.556
  222.4 8.3 %rev.29 = bf16[512,512]{1,0:T(8,128)(2,1)} reverse(bf16[512,512]{1,0:T(8,128)(2,1)} %bitcast.312), dimensions={0} | reverse | bytes 1048576 | tf_op jit(solution)/shard_map/rev | solution.py:271
  230.7 2.9 reshape.557
  233.6 2.3 copy.204
  236.2 2.0 copy.200
  239.3 2.8 fusion.164
  243.3 4.4 %rev.33 = bf16[512,256]{1,0:T(8,128)(2,1)} reverse(bf16[512,256]{1,0:T(8,128)(2,1)} %bitcast.317), dimensions={0} | reverse | bytes 524288 | tf_op jit(solution)/shard_map/rev | solution.py:180
  247.7 2.1 reshape.551
  250.9 3.7 fusion.77
  254.6 1.6 broadcast.242.clone
  256.2 8.1 %while.27 = (s32[]{:T(128)}, f32[2,4,128,64]{3,2,1,0:T(8,128)S(1)}, f32[4,2,4,128,64]{4,3,2,1,0:T(8,128)}, f32[4,2,4]{2,1,0:T(2,128)S(1)}, f32[4,2,4,128,64]{4,3,2,1,0:T(8,128)}, /*index=5*/s32[]{:T(128)}, s32[]{:T(128)}) while((s32[]{:T(128)}, f32[2,4,128,64]{3,2,1,0:T(8,128)S(1)}, f32[4,2,4,128,64]{4,3,2,1,0:T(8,128)}, ...), condition=%wide.region_18.19_spmd.clone, body=%wide.region_17.18_spmd.clone.sunk | while | flops 262147 | bytes 1573068 | solution.py:71
  266.1 16.2 %all_gather.27 = bf16[4,8,128,64]{2,3,1,0:T(8,128)(2,1)S(1)} all-gather(bf16[1,8,128,64]{2,3,1,0:T(8,128)(2,1)S(1)} %bitcast.323), channel_id=1, replica_groups=mesh['sp'=4,'tp'=4,'dp'=2] {'sp'}, dimensions={0}, use_global_device_ids=true | all-gather | bytes 655360 | tf_op jit(solution)/shard_map/all_gather | solution.py:237
  285.3 2.8 fusion.50
  290.9 2.3 convolution_bitcast_fusion
  293.2 1.9 fusion.42
  296.9 9.4 %rev.37 = f32[512,512]{0,1:T(8,128)} reverse(f32[512,512]{0,1:T(8,128)} %bitcast.314), dimensions={0} | reverse | bytes 2097152 | tf_op jit(solution)/shard_map/rev | solution.py:270
  306.3 1.6 copy.183
  308.1 2.9 convolution_bitcast_fusion.1
  311.0 2.5 fusion.76
  313.5 1.6 broadcast.242.clone.1
  315.1 8.2 %while.26 = (s32[]{:T(128)}, f32[2,4,128,64]{3,2,1,0:T(8,128)S(1)}, f32[4,2,4,128,64]{4,3,2,1,0:T(8,128)}, f32[4,2,4]{2,1,0:T(2,128)S(1)}, f32[4,2,4,128,64]{4,3,2,1,0:T(8,128)}, /*index=5*/s32[]{:T(128)}, s32[]{:T(128)}) while((s32[]{:T(128)}, f32[2,4,128,64]{3,2,1,0:T(8,128)S(1)}, f32[4,2,4,128,64]{4,3,2,1,0:T(8,128)}, ...), condition=%wide.region_7.8_spmd.clone, body=%wide.region_6.7_spmd.clone.sunk | while | flops 262147 | bytes 1573068 | solution.py:71
  323.5 15.8 %all_gather.23 = bf16[4,8,128,64]{2,3,1,0:T(8,128)(2,1)S(1)} all-gather(bf16[1,8,128,64]{2,3,1,0:T(8,128)(2,1)S(1)} %bitcast.324), channel_id=1, replica_groups=mesh['sp'=4,'tp'=4,'dp'=2] {'sp'}, dimensions={0}, use_global_device_ids=true | all-gather | bytes 655360 | tf_op jit(solution)/shard_map/all_gather | solution.py:231
  339.6 3.6 fusion.52
  344.6 3.9 fusion.33
  350.1 1.6 bitcast_reduce_fusion
  351.9 2.6 convolution_convert_fusion
  354.6 34.4 %reduce-scatter.2.cloned.1.call-done = bf16[128,2048]{1,0:T(8,128)(2,1)} async-done(((bf16[512,2048]{1,0:T(8,128)(2,1)}), bf16[128,2048]{1,0:T(8,128)(2,1)}) %reduce-scatter.2.cloned.1.call-update) | async-done | bytes 524304 | tf_op jit(solution)/shard_map/reduce_scatter | solution.py:284
  389.0 2.0 fusion.122
  (177 shorter events, 54.0 us)
Async XLA Ops:
  6.5 345.4 %copy-start = (bf16[512,2048]{1,0:T(8,128)(2,1)S(1)}, bf16[512,2048]{1,0:T(8,128)(2,1)}, u32[]{:S(2)}) copy-start(bf16[512,2048]{1,0:T(8,128)(2,1)} %param.41) | copy-start | bytes 6291460
  6.5 143.6 %all-gather.5.cloned.1.call-start = ((), (), s32[]{:S(2)}) async-start(), calls=%async_computation.2 | async-start | bytes 1310720 | tf_op jit(solution)/shard_map/all_gather | solution.py:193
  6.5 4.6 %copy-start.4 = (bf16[1,256,2048]{2,1,0:T(8,128)(2,1)S(1)}, bf16[1,256,2048]{2,1,0:T(8,128)(2,1)}, u32[]{:S(2)}) copy-start(bf16[1,256,2048]{2,1,0:T(8,128)(2,1)} %param.25) | copy-start | bytes 3145732
  91.2 3.5 copy-start.1
  94.6 1.9 copy-start.25
  94.6 3.1 copy-start.22
  94.7 64.9 %all-gather.3.cloned.1.call-start = ((), (), s32[]{:S(2)}) async-start(), calls=%async_computation.1 | async-start | bytes 2621440 | tf_op jit(solution)/shard_map/all_gather | solution.py:141
  96.4 292.5 %reduce-scatter.2.cloned.1.call-start = ((), (), s32[]{:S(2)}) async-start(), calls=%async_computation.3 | async-start | bytes 2621440 | tf_op jit(solution)/shard_map/reduce_scatter | solution.py:284
  150.1 1.6 copy-start.5
  161.8 24.1 %copy-start.12 = (f32[512,2,8]{0,2,1:T(8,128)}, f32[512,2,8]{0,2,1:T(8,128)S(1)}, u32[]{:S(2)}) copy-start(f32[512,2,8]{0,2,1:T(8,128)S(1)} %bitcast_convert_fusion.1) | copy-start | bytes 98308
  190.7 12.0 %slice-start = ((f32[512,2,8]{0,2,1:T(8,128)}), f32[512,1,8]{0,2,1:T(8,128)S(1)}, s32[]{:S(2)}) async-start(f32[512,2,8]{0,2,1:T(8,128)} %copy-done.12), calls=%async_computation.4 | async-start | bytes 32768 | tf_op jit(solution)/shard_map/slice | solution.py:172
  236.2 5.9 %copy-start.14 = (f32[512,8]{0,1:T(8,128)}, f32[512,8]{0,1:T(8,128)S(1)}, u32[]{:S(2)}) copy-start(f32[512,8]{0,1:T(8,128)S(1)} %rev.32) | copy-start | bytes 49156
  285.2 5.1 %copy-start.6 = (bf16[8,64,256]{2,1,0:T(8,128)(2,1)S(1)}, bf16[8,64,256]{2,1,0:T(8,128)(2,1)}, u32[]{:S(2)}) copy-start(bf16[8,64,256]{2,1,0:T(8,128)(2,1)} %multiply_convert_fusion.23) | copy-start | bytes 786436
  285.3 5.6 %copy-start.15 = (f32[512,8]{0,1:T(8,128)S(1)}, f32[512,8]{0,1:T(8,128)}, u32[]{:S(2)}) copy-start(f32[512,8]{0,1:T(8,128)} %copy-done.14) | copy-start | bytes 49156
  285.3 5.6 %copy-start.18 = (f32[4,128,2,4]{1,3,2,0:T(4,128)S(1)}, f32[4,128,2,4]{1,3,2,0:T(4,128)}, u32[]{:S(2)}) copy-start(f32[4,128,2,4]{1,3,2,0:T(4,128)} %copy.202) | copy-start | bytes 49156
  285.3 5.6 %copy-start.19 = (pred[128,128]{1,0:T(8,128)(4,1)S(1)}, pred[128,128]{1,0:T(8,128)(4,1)}, u32[]{:S(2)}) copy-start(pred[128,128]{1,0:T(8,128)(4,1)} %iota_compare_fusion) | copy-start | bytes 49156
  290.8 2.3 copy-start.3
  290.8 2.3 copy-start.10
  290.9 2.3 copy-start.21
  296.9 11.0 %copy-start.13 = (f32[4,128,2,4]{1,3,2,0:T(4,128)S(1)}, f32[4,128,2,4]{1,3,2,0:T(4,128)}, u32[]{:S(2)}) copy-start(f32[4,128,2,4]{1,3,2,0:T(4,128)} %copy.181) | copy-start | bytes 49156
  296.9 11.0 %copy-start.16 = (f32[4,2,4]{2,1,0:T(2,128)S(1)}, f32[4,2,4]{2,1,0:T(2,128)}, u32[]{:S(2)}) copy-start(f32[4,2,4]{2,1,0:T(2,128)} %slice_bitcast_fusion.4) | copy-start | bytes 388
  308.1 2.9 copy-start.9
  323.3 16.3 %copy-start.17 = (f32[1024,2,4]{0,2,1:T(4,128)S(1)}, f32[1024,2,4]{0,2,1:T(4,128)}, u32[]{:S(2)}) copy-start(f32[1024,2,4]{0,2,1:T(4,128)} %mul.778) | copy-start | bytes 98308
  339.4 5.0 %copy-start.8 = (f32[4,128,2,4]{3,2,1,0:T(2,128)S(1)}, f32[4,128,2,4]{3,2,1,0:T(2,128)}, u32[]{:S(2)}) copy-start(f32[4,128,2,4]{3,2,1,0:T(2,128)} %exp.175) | copy-start | bytes 49156
  339.6 5.0 %copy-start.20 = (f32[4,2,4]{2,1,0:T(2,128)S(1)}, f32[4,2,4]{2,1,0:T(2,128)}, u32[]{:S(2)}) copy-start(f32[4,2,4]{2,1,0:T(2,128)} %fusion.54) | copy-start | bytes 388
  344.6 4.6 %copy-start.11 = (f32[512,512]{0,1:T(8,128)S(1)}, f32[512,512]{0,1:T(8,128)}, u32[]{:S(2)}) copy-start(f32[512,512]{0,1:T(8,128)} %rev.37) | copy-start | bytes 3145732
  344.6 4.6 %copy-start.26 = (bf16[2048,512]{1,0:T(8,128)(2,1)S(1)}, bf16[2048,512]{1,0:T(8,128)(2,1)}, u32[]{:S(2)}) copy-start(bf16[2048,512]{1,0:T(8,128)(2,1)} %param.31) | copy-start | bytes 6291460
  348.5 1.6 copy-start.7
  350.1 1.6 copy-start.24
  354.6 34.4 %copy-start.2 = (bf16[1,128,2048]{2,1,0:T(8,128)(2,1)S(1)}, bf16[1,128,2048]{2,1,0:T(8,128)(2,1)}, u32[]{:S(2)}) copy-start(bf16[1,128,2048]{2,1,0:T(8,128)(2,1)} %param.23) | copy-start | bytes 1572868
  354.6 34.4 %copy-start.23 = (f32[2048]{0:T(1024)S(1)}, f32[2048]{0:T(1024)}, u32[]{:S(2)}) copy-start(f32[2048]{0:T(1024)} %get-tuple-element.173) | copy-start | bytes 24580
Sparse Core Ops, SparseCore 0:
  94.8 28.3 all-gather.4
  125.0 34.4 all-gather.2
  354.7 34.1 reduce-scatter.1
where the time goes:
time: 402 us; the launch traced here: 397 us
  blocking collectives  154 us (38%)
  local copies, waits for them, and re-layouts  87.3 us (22%)
  other arithmetic  53.5 us (13%)
  matrix products  51.8 us (13%)
  waiting for transfers between devices  37.3 us (9%)
  between operations  13.7 us (3%)
    psum x1, blocking collectives, per_device(): lax.psum((shift_part, scale_part, gate_part), ('sp', 'tp'))  79.3 us
    reduce_scatter x1, waiting for transfers between devices, per_device(): lax.psum_scatter(jnp.dot(inner_rows, out_proj, preferred_element_type=jnp...  34.4 us
    all_gather x1, blocking collectives, per_device(): lax.all_gather(backward_end.reshape(1, heads_dev, STATE, HEAD).astype(jnp...  16.2 us
    all_gather x1, blocking collectives, per_device(): lax.all_gather(forward_end.reshape(1, heads_dev, STATE, HEAD).astype(jnp....  15.8 us
    all_gather x1, blocking collectives, per_device(): lax.all_gather(context_write, 'sp', axis=0, tiled=True)  14.7 us
    all_gather x1, blocking collectives, per_device(): lax.all_gather(step_raw, 'sp', axis=0, tiled=True)  14.1 us
    all_gather x1, blocking collectives, per_device(): lax.all_gather(context_raw, 'sp', axis=0, tiled=True)  13.4 us
    convert_element_type x5, local copies, waits for them, and re-layouts, convolve(): return jax.nn.silu(summed).reshape(length, channels).astype(jnp.bfloat16)  9.56 us
  transfers between devices with their start and end apart: 3, of which 2 were waited for; matrix products, arithmetic and copies ran while one was open for 8% of the time, Pallas kernels for 0%

commit v1 on v0

v1 whole, which is shorter than its diff:
```python
import functools

import jax
import jax.numpy as jnp
from jax import lax
from jax.experimental import pallas as pl
from jax.experimental.pallas import tpu as pltpu
from jax.sharding import PartitionSpec as P

HEAD = 64
STATE = 128
ROW = 64
BLOCK = 128
LANES = 128
HALO = 16

NORM_FLOOR = 1e-05
GATED_FLOOR = 1e-06
FINEST = lax.Precision.HIGHEST
MESH = pl.DeviceIdType.MESH
F32 = jnp.float32
BF16 = jnp.bfloat16


def vmem():
    return pl.BlockSpec(memory_space=pltpu.VMEM)


def send(src, dst, send_sem, recv_sem, axis, target):
    copy = pltpu.make_async_remote_copy(
        src_ref=src,
        dst_ref=dst,
        send_sem=send_sem,
        recv_sem=recv_sem,
        device_id={axis: target},
        device_id_type=MESH,
    )
    copy.start()
    return copy


def greet(peers):
    barrier = pltpu.get_barrier_semaphore()
    for axis, target in peers:
        pl.semaphore_signal(barrier, inc=1, device_id={axis: target}, device_id_type=MESH)
    pl.semaphore_wait(barrier, len(peers))


def others(axis, count):
    me = lax.axis_index(axis)
    return [lax.rem(me + d, count) for d in range(1, count)]


def spread_kernel(
    sp_n, tp_n,
    act, shift_m, scale_m, gate_m, latent, context,
    latent_all, context_ext, mod,
    part, tp_box, middle, sp_box,
    lat_s, lat_r, tps, tpr, sps, spr, halo_s, halo_r, own,
):
    sp, tp = lax.axis_index("sp"), lax.axis_index("tp")
    tp_peers, sp_peers = others("tp", tp_n), others("sp", sp_n)
    rows, ctx_rows = latent.shape[0], context.shape[0]
    greet([("tp", p) for p in tp_peers] + [("sp", p) for p in sp_peers])
    mine = pl.ds(pl.multiple_of(tp * rows, rows), rows)
    copy_lat = pltpu.make_async_copy(latent, latent_all.at[mine], own.at[0])
    copy_lat.start()
    copy_ctx = pltpu.make_async_copy(context, context_ext.at[pl.ds(HALO, ctx_rows)], own.at[1])
    copy_ctx.start()
    before = lax.rem(sp + sp_n - 1, sp_n)
    after = lax.rem(sp + 1, sp_n)
    halos = [
        send(context.at[pl.ds(ctx_rows - HALO, HALO)], context_ext.at[pl.ds(0, HALO)],
             halo_s.at[0], halo_r.at[0], "sp", after),
        send(context.at[pl.ds(0, HALO)], context_ext.at[pl.ds(HALO + ctx_rows, HALO)],
             halo_s.at[1], halo_r.at[1], "sp", before),
    ]
    total = jnp.dot(act[0:16, :], shift_m[...], preferred_element_type=F32)
    total += jnp.dot(act[16:32, :], scale_m[...], preferred_element_type=F32)
    total += jnp.dot(act[32:48, :], gate_m[...], preferred_element_type=F32)
    part[...] = total[0:8]
    first = [
        send(part, tp_box.at[d], tps.at[d], tpr.at[d], "tp", p) for d, p in enumerate(tp_peers)
    ]
    rows_out = [
        send(latent, latent_all.at[mine], lat_s.at[d], lat_r.at[d], "tp", p)
        for d, p in enumerate(tp_peers)
    ]
    for copy in first:
        copy.wait()
    summed = part[...]
    for d in range(tp_n - 1):
        summed += tp_box[d]
    middle[...] = summed
    second = [
        send(middle, sp_box.at[d], sps.at[d], spr.at[d], "sp", p) for d, p in enumerate(sp_peers)
    ]
    for copy in second:
        copy.wait()
    summed = middle[...]
    for d in range(sp_n - 1):
        summed += sp_box[d]
    mod[...] = summed
    for copy in halos:
        copy.wait()
    copy_lat.wait()
    copy_ctx.wait()
    for copy in rows_out:
        copy.wait()


def softplus(x):
    return jnp.maximum(x, 0.0) + jnp.log1p(jnp.exp(-jnp.abs(x)))


def silu(x):
    return x * (1.0 / (1.0 + jnp.exp(-x)))


def modulate_into(source, target, shift_row, scale_row):
    step = 16

    def tile(i, carry):
        at = pl.ds(pl.multiple_of(i * step, step), step)
        values = source[at, :].astype(F32)
        center = jnp.mean(values, -1, keepdims=True)
        values = values - center
        spread = jnp.mean(values * values, -1, keepdims=True)
        normed = values * lax.rsqrt(spread + NORM_FLOOR)
        target[at, :] = (normed * (1.0 + scale_row[...]) + shift_row[...]).astype(BF16)
        return carry

    lax.fori_loop(0, source.shape[0] // step, tile, 0)


def conv_silu(values, taps, run):
    rows, channels = values.shape
    margin = taps.shape[0] // 2
    place = lax.broadcasted_iota(jnp.int32, (rows, channels), 0) % run
    summed = jnp.zeros((rows, channels), F32)
    for k in range(taps.shape[0]):
        offset = k - margin
        moved = pltpu.roll(values, (-offset) % rows, 0) if offset else values
        if offset:
            moved = jnp.where((place + offset >= 0) & (place + offset < run), moved, 0.0)
        summed += moved * taps[k : k + 1, :]
    return silu(summed).astype(BF16)


def running(decay, heads):
    rows = decay.shape[0]
    at = lax.broadcasted_iota(jnp.int32, (rows, rows), 0)
    by = lax.broadcasted_iota(jnp.int32, (rows, rows), 1)
    lower = (by <= at).astype(F32)
    upper = (by >= at).astype(F32)
    lane = lax.broadcasted_iota(jnp.int32, decay.shape, 1)
    forward = jnp.dot(lower, decay, precision=FINEST, preferred_element_type=F32)
    backward = jnp.dot(upper, decay, precision=FINEST, preferred_element_type=F32)
    return jnp.where(lane < heads, forward, backward)


def lane_to_rows(row, count):
    return jnp.broadcast_to(row, (LANES, LANES)).T[0:count]


def partial_states(values, writes, weight, heads, per_group):
    turned = values.astype(F32).T.astype(BF16)
    result = []
    for h in range(heads):
        g = h // per_group
        rows = writes[:, g * STATE : (g + 1) * STATE].astype(F32)
        pair = jnp.concatenate(
            [(rows * weight[:, h : h + 1]).astype(BF16),
             (rows * weight[:, heads + h : heads + h + 1]).astype(BF16)], axis=1)
        result.append(
            jnp.dot(turned[h * HEAD : (h + 1) * HEAD], pair, preferred_element_type=F32))
    return result


def project_kernel(
    sp_n, heads, per_group,
    latent, context_ext, mod, value_p, gate_p, write_p, read_p, step_p,
    rates, pacing, value_t, write_t, read_t,
    values_o, gate_o, writes_o, reads_o, step_o, cumul_o, inc_o, states_o, tots_o,
    hidden, hidden_c, ctx_v, ctx_w,
):
    sp, tp = lax.axis_index("sp"), lax.axis_index("tp")
    tokens = latent.shape[0]
    ext = context_ext.shape[0]
    ctx_rows = ext - 2 * HALO
    width, keys = value_p.shape[1], write_p.shape[1]
    blocks = tokens // BLOCK
    piece = 256
    modulate_into(latent, hidden, mod.at[0:1, :], mod.at[2:3, :])
    modulate_into(context_ext, hidden_c, mod.at[1:2, :], mod.at[3:4, :])

    def taps_at(ref, start):
        return ref[:, pl.ds(pl.multiple_of(start, piece), piece)]

    place = lax.broadcasted_iota(jnp.int32, (ext, piece), 0)
    live = ((place >= HALO) | (sp > 0)) & ((place < HALO + ctx_rows) | (sp < sp_n - 1))

    def latent_part(weight, taps, total, out):
        for c in range(0, total, piece):
            pre = jnp.dot(hidden[...], weight[:, c : c + piece], preferred_element_type=F32)
            pre = pre.astype(BF16)
            if taps is None:
                out[:, c : c + piece] = pre
            else:
                kernel = taps_at(taps, tp * total + c)
                out[:, c : c + piece] = conv_silu(pre.astype(F32), kernel, ROW)

    def context_part(weight, taps, total, out):
        for c in range(0, total, piece):
            pre = jnp.dot(hidden_c[...], weight[:, c : c + piece], preferred_element_type=F32)
            pre = jnp.where(live, pre.astype(BF16).astype(F32), 0.0)
            done = conv_silu(pre, taps_at(taps, tp * total + c), ext)
            out[:, c : c + piece] = done[HALO : HALO + ctx_rows]

    latent_part(value_p, value_t, width, values_o)
    latent_part(gate_p, None, width, gate_o)
    latent_part(write_p, write_t, keys, writes_o)
    latent_part(read_p, read_t, keys, reads_o)
    context_part(value_p, value_t, width, ctx_v)
    context_part(write_p, write_t, keys, ctx_w)
    raw = jnp.dot(hidden[...], step_p[...], preferred_element_type=F32).astype(BF16)
    pace = pacing[:, pl.ds(pl.multiple_of(sp * tokens, tokens), tokens)]
    pace = jnp.broadcast_to(pace, (LANES, tokens)).T
    step_o[...] = softplus(raw.astype(F32)) * pace
    raw_c = jnp.dot(hidden_c[...], step_p[...], preferred_element_type=F32).astype(BF16)
    step_c = softplus(raw_c.astype(F32))[HALO : HALO + ctx_rows]
    rate = rates[0:1, :]

    grand = jnp.zeros((1, LANES), F32)
    drops = []
    for k in range(blocks):
        at = slice(k * BLOCK, (k + 1) * BLOCK)
        step = step_o[at, :]
        decay = -rate * step
        cumul = running(decay, heads)
        total = jnp.sum(decay, axis=0, keepdims=True)
        cumul_o[at, :] = cumul
        weight = jnp.exp(total - cumul) * step
        grand += total
        drops.append(jnp.exp(total))
        found = partial_states(values_o[at, :], writes_o[at, :], weight, heads, per_group)
        for h in range(heads):
            inc_o[k, h * HEAD : (h + 1) * HEAD, :] = found[h]
    for h in range(heads):
        rows = slice(h * HEAD, (h + 1) * HEAD)
        forward = inc_o[0, rows, 0:STATE]
        for k in range(1, blocks):
            forward = drops[k][:, h : h + 1] * forward + inc_o[k, rows, 0:STATE]
        backward = inc_o[blocks - 1, rows, STATE : 2 * STATE]
        for k in range(blocks - 2, -1, -1):
            backward = (
                drops[k][:, heads + h : heads + h + 1] * backward
                + inc_o[k, rows, STATE : 2 * STATE])
        states_o[0, rows, :] = forward.astype(BF16)
        states_o[1, rows, :] = backward.astype(BF16)
    decay_c = -rate * step_c
    total_c = jnp.sum(decay_c, axis=0, keepdims=True)
    weight_c = jnp.exp(total_c - running(decay_c, heads)) * step_c
    found = partial_states(ctx_v[...], ctx_w[...], weight_c, heads, per_group)
    for h in range(heads):
        rows = slice(h * HEAD, (h + 1) * HEAD)
        states_o[2, rows, :] = found[h][:, 0:STATE].astype(BF16)
        states_o[3, rows, :] = found[h][:, STATE : 2 * STATE].astype(BF16)
    tots_o[0 : 2 * heads, :] = lane_to_rows(grand, 2 * heads)
    tots_o[2 * heads : 4 * heads, :] = lane_to_rows(total_c, 2 * heads)


def states_kernel(
    sp_n, heads,
    states, tots,
    starts,
    box, tot_box, outgoing,
    s1, r1, s2, r2, s3, r3,
):
    sp = lax.axis_index("sp")
    peers = others("sp", sp_n)
    share = states.shape[1] // sp_n
    greet([("sp", p) for p in peers])

    def rows_of(p):
        return pl.ds(pl.multiple_of(p * share, share), share)

    copies = []
    for d, p in enumerate(peers):
        copies.append(send(tots, tot_box.at[sp], s2.at[d], r2.at[d], "sp", p))
        copies.append(send(states.at[:, rows_of(p), :], box.at[sp], s1.at[d], r1.at[d], "sp", p))
    box[sp] = states[:, rows_of(sp), :]
    tot_box[sp] = tots[...]
    for copy in copies:
        copy.wait()
    first = (sp * share) // HEAD
    each = min(HEAD, share)

    def factor(j, base):
        rows = [
            jnp.broadcast_to(jnp.exp(tot_box[j, pl.ds(base + first + q, 1), :]), (each, STATE))
            for q in range(max(1, share // HEAD))
        ]
        return rows[0] if len(rows) == 1 else jnp.concatenate(rows, axis=0)

    forward = jnp.zeros((share, STATE), F32)
    for j in range(sp_n):
        forward = factor(j, 2 * heads) * forward + box[j, 2].astype(F32)
    backward = jnp.zeros((share, STATE), F32)
    for j in range(sp_n - 1, -1, -1):
        backward = factor(j, 3 * heads) * backward + box[j, 3].astype(F32)
    for j in range(sp_n):
        outgoing[j, 0] = forward.astype(BF16)
        forward = factor(j, 0) * forward + box[j, 0].astype(F32)
    for j in range(sp_n - 1, -1, -1):
        outgoing[j, 1] = backward.astype(BF16)
        backward = factor(j, heads) * backward + box[j, 1].astype(F32)
    back = [
        send(outgoing.at[p], starts.at[:, rows_of(sp), :], s3.at[d], r3.at[d], "sp", p)
        for d, p in enumerate(peers)
    ]
    starts[:, rows_of(sp), :] = outgoing[sp]
    for copy in back:
        copy.wait()


def sweep_kernel(
    heads, per_group,
    values, gate, writes, reads, step, cumul, inc, starts, gain, out_p,
    mixed_o,
    state_f, state_b, inner, joined,
):
    tp = lax.axis_index("tp")
    tokens = values.shape[0]
    width = values.shape[1]
    blocks = tokens // BLOCK
    span = per_group * HEAD
    groups = heads // per_group
    drops = [
        jnp.exp(jnp.where(
            lax.broadcasted_iota(jnp.int32, (1, LANES), 1) < heads,
            cumul[(k + 1) * BLOCK - 1 : (k + 1) * BLOCK, :],
            cumul[k * BLOCK : k * BLOCK + 1, :]))
        for k in range(blocks)
    ]
    for h in range(heads):
        rows = slice(h * HEAD, (h + 1) * HEAD)
        forward = starts[0, rows, :].astype(F32)
        for k in range(blocks):
            state_f[k, rows, :] = forward.astype(BF16)
            forward = drops[k][:, h : h + 1] * forward + inc[k, rows, 0:STATE]
        backward = starts[1, rows, :].astype(F32)
        for k in range(blocks - 1, -1, -1):
            state_b[k, rows, :] = backward.astype(BF16)
            backward = (
                drops[k][:, heads + h : heads + h + 1] * backward
                + inc[k, rows, STATE : 2 * STATE])
    at = lax.broadcasted_iota(jnp.int32, (BLOCK, BLOCK), 0)
    by = lax.broadcasted_iota(jnp.int32, (BLOCK, BLOCK), 1)
    past, diagonal = by <= at, by == at
    contract = (((1,), (1,)), ((), ()))

    def one_block(k, carry):
        rows = pl.ds(pl.multiple_of(k * BLOCK, BLOCK), BLOCK)
        c = cumul[rows, :]
        s = step[rows, :]
        c_turned, s_turned = c.T, s.T
        grown = jnp.exp(c)
        turned = values[rows, :].astype(F32).T.astype(BF16)
        for g in range(groups):
            read = reads[rows, g * STATE : (g + 1) * STATE]
            write = writes[rows, g * STATE : (g + 1) * STATE]
            affinity = lax.dot_general(read, write, contract, preferred_element_type=F32)
            read = read.astype(F32)
            for r in range(per_group):
                h = g * per_group + r
                b = heads + h
                head = slice(h * HEAD, (h + 1) * HEAD)
                exponent = jnp.where(
                    past,
                    c[:, h : h + 1] - c_turned[h : h + 1, :],
                    c[:, b : b + 1] - c_turned[b : b + 1, :])
                fs, bs = s_turned[h : h + 1, :], s_turned[b : b + 1, :]
                steps = jnp.where(past, fs, bs) + jnp.where(diagonal, bs, 0.0)
                mixing = (affinity * jnp.exp(exponent) * steps).astype(BF16)
                left = jnp.concatenate(
                    [mixing,
                     (read * grown[:, h : h + 1]).astype(BF16),
                     (read * grown[:, b : b + 1]).astype(BF16)], axis=1)
                right = jnp.concatenate(
                    [turned[head], state_f[k, head, :], state_b[k, head, :]], axis=1)
                joined[:, head] = lax.dot_general(
                    left, right, contract, preferred_element_type=F32)
            lanes = slice(g * span, (g + 1) * span)
            gated = joined[:, lanes] * silu(gate[rows, lanes].astype(F32))
            scale = lax.rsqrt(jnp.mean(gated * gated, -1, keepdims=True) + GATED_FLOOR)
            start = pl.multiple_of(tp * width + g * span, span)
            inner[rows, lanes] = (gated * scale * gain[:, pl.ds(start, span)]).astype(BF16)
        return carry

    lax.fori_loop(0, blocks, one_block, 0)
    piece = 512
    for c in range(0, out_p.shape[1], piece):
        mixed_o[:, c : c + piece] = jnp.dot(
            inner[...], out_p[:, c : c + piece], preferred_element_type=F32).astype(BF16)


def finish_kernel(tp_n, mixed, latent, mod, updated, box, ss, rs):
    tp = lax.axis_index("tp")
    peers = others("tp", tp_n)
    rows = latent.shape[0]
    greet([("tp", p) for p in peers])
    copies = [
        send(mixed.at[pl.ds(pl.multiple_of(p * rows, rows), rows)], box.at[d],
             ss.at[d], rs.at[d], "tp", p)
        for d, p in enumerate(peers)
    ]
    for copy in copies:
        copy.wait()
    tile_rows = 16

    def tile(i, carry):
        at = pl.ds(pl.multiple_of(i * tile_rows, tile_rows), tile_rows)
        own = pl.ds(pl.multiple_of(tp * rows + i * tile_rows, tile_rows), tile_rows)
        total = mixed[own, :].astype(F32)
        for d in range(tp_n - 1):
            total += box[d, at, :].astype(F32)
        total = total.astype(BF16).astype(F32)
        updated[at, :] = (latent[at, :].astype(F32) + mod[4:5, :] * total).astype(BF16)
        return carry

    lax.fori_loop(0, rows // tile_rows, tile, 0)


def shape(dims, kind):
    return jax.ShapeDtypeStruct(dims, kind)


def call(body, outs, count, scratch, collective=None, limit=60 << 20):
    params = dict(vmem_limit_bytes=limit)
    if collective is not None:
        params.update(collective_id=collective, has_side_effects=True)
    single = not isinstance(outs, (list, tuple))
    return pl.pallas_call(
        body,
        out_shape=outs,
        in_specs=[vmem()] * count,
        out_specs=vmem() if single else [vmem()] * len(outs),
        scratch_shapes=scratch,
        compiler_params=pltpu.CompilerParams(**params),
    )


def dma(count):
    return pltpu.SemaphoreType.DMA((count,))


def per_device(
    sp_n, tp_n,
    latent, condition, context, context_cond, shift_matrix, scale_matrix, gate_matrix,
    value_proj, gate_proj, write_proj, read_proj, step_proj, decay_rate, pacing,
    value_taps, write_taps, read_taps, norm_gain, out_proj,
):
    sp, tp = lax.axis_index("sp"), lax.axis_index("tp")
    rows, model = latent.shape[1:]
    ctx_rows = context.shape[1]
    tokens = rows * tp_n
    width, keys = value_proj.shape[1], write_proj.shape[1]
    heads = width // HEAD
    per_group = heads // (keys // STATE)
    blocks = tokens // BLOCK
    row_share = shift_matrix.shape[0]

    pair = jnp.stack([condition[0], context_cond])
    pair = lax.dynamic_slice_in_dim(pair, (sp * tp_n + tp) * row_share, row_share, 1)
    pair = jax.nn.silu(pair).astype(BF16)
    act = jnp.concatenate([
        jnp.pad(pair, ((0, 14), (0, 0))),
        jnp.pad(pair, ((2, 12), (0, 0))),
        jnp.pad(pair[:1], ((4, 11), (0, 0))),
    ])
    step_cols = lax.dynamic_slice_in_dim(step_proj, tp * heads, heads, 2)
    step_cols = jnp.pad(step_cols.reshape(model, 2 * heads), ((0, 0), (0, LANES - 2 * heads)))
    rates = lax.dynamic_slice_in_dim(decay_rate, tp * heads, heads, 1).reshape(1, 2 * heads)
    rates = jnp.pad(rates, ((0, 7), (0, LANES - 2 * heads)))

    latent_all, context_ext, mod = call(
        functools.partial(spread_kernel, sp_n, tp_n),
        [shape((tokens, model), BF16), shape((ctx_rows + 2 * HALO, model), BF16),
         shape((8, model), F32)],
        6,
        [pltpu.VMEM((8, model), F32), pltpu.VMEM((tp_n - 1, 8, model), F32),
         pltpu.VMEM((8, model), F32), pltpu.VMEM((sp_n - 1, 8, model), F32),
         dma(tp_n), dma(tp_n), dma(tp_n), dma(tp_n), dma(sp_n), dma(sp_n), dma(2), dma(2),
         dma(2)],
        0,
    )(act, shift_matrix, scale_matrix, gate_matrix, latent[0], context[0])

    values, gate, writes, reads, step, cumul, inc, states, tots = call(
        functools.partial(project_kernel, sp_n, heads, per_group),
        [shape((tokens, width), BF16), shape((tokens, width), BF16),
         shape((tokens, keys), BF16), shape((tokens, keys), BF16),
         shape((tokens, LANES), F32), shape((tokens, LANES), F32),
         shape((blocks, width, 2 * STATE), F32), shape((4, width, STATE), BF16),
         shape((4 * heads, LANES), F32)],
        13,
        [pltpu.VMEM((tokens, model), BF16), pltpu.VMEM((ctx_rows + 2 * HALO, model), BF16),
         pltpu.VMEM((ctx_rows, width), BF16), pltpu.VMEM((ctx_rows, keys), BF16)],
    )(latent_all, context_ext, mod, value_proj, gate_proj, write_proj, read_proj, step_cols,
      rates, pacing, value_taps, write_taps, read_taps)

    share = width // sp_n
    starts = call(
        functools.partial(states_kernel, sp_n, heads),
        shape((2, width, STATE), BF16),
        2,
        [pltpu.VMEM((sp_n, 4, share, STATE), BF16), pltpu.VMEM((sp_n, 4 * heads, LANES), F32),
         pltpu.VMEM((sp_n, 2, share, STATE), BF16),
         dma(sp_n), dma(sp_n), dma(sp_n), dma(sp_n), dma(sp_n), dma(sp_n)],
        1,
    )(states, tots)

    mixed = call(
        functools.partial(sweep_kernel, heads, per_group),
        shape((tokens, model), BF16),
        10,
        [pltpu.VMEM((blocks, width, STATE), BF16), pltpu.VMEM((blocks, width, STATE), BF16),
         pltpu.VMEM((tokens, width), BF16), pltpu.VMEM((BLOCK, width), F32)],
    )(values, gate, writes, reads, step, cumul, inc, starts, norm_gain[None], out_proj)

    updated = call(
        functools.partial(finish_kernel, tp_n),
        shape((rows, model), BF16),
        3,
        [pltpu.VMEM((tp_n - 1, rows, model), BF16), dma(tp_n), dma(tp_n)],
        2,
    )(mixed, latent[0], mod)
    return updated[None]


def solution(mesh):
    placed = (
        P("dp", ("sp", "tp"), None),
        P("dp", None),
        P("dp", "sp", None),
        P(),
        P(("sp", "tp"), None),
        P(("sp", "tp"), None),
        P(("sp", "tp"), None),
        P(None, "tp"),
        P(None, "tp"),
        P(None, "tp"),
        P(None, "tp"),
        P(),
        P(),
        P("dp", None),
        P(),
        P(),
        P(),
        P(),
        P("tp", None),
    )
    return jax.shard_map(
        functools.partial(per_device, mesh.shape["sp"], mesh.shape["tp"]),
        mesh=mesh,
        in_specs=placed,
        out_specs=P("dp", ("sp", "tp"), None),
        check_vma=False,
    )
```

time: 402 us -> 132 us (0.33)
  blocking collectives: 154 us -> 0 us
  Pallas kernels: 0 us -> 125 us
  local copies, waits for them, and re-layouts: 87.3 us -> 4.51 us
  other arithmetic: 53.5 us -> 1.4 us
  matrix products: 51.8 us -> 0 us
  waiting for transfers between devices: 37.3 us -> 0 us
  between operations: 13.7 us -> 0.04 us
    pallas_call x0 -> x5, Pallas kernels: none -> 125 us  [the longest x1 36.6 us: per_device(): call(functools.partial(spread_kernel, sp_n, tp_n), [shape((tokens, model)...]
    psum x1 -> x0, blocking collectives: 79.3 us -> none  [per_device(): lax.psum((shift_part, scale_part, gate_part), ('sp', 'tp'))]
    all_gather x5 -> x0, blocking collectives: 74.3 us -> none  [the longest x1 16.2 us: per_device(): lax.all_gather(backward_end.reshape(1, heads_dev, STATE, HEAD).astype(jnp...]
    dot_general x21 -> x0, matrix products: 51.8 us -> none  [the longest x2 6.44 us: context_state(): jnp.einsum('lgrn,lgrp->grnp', scaled, head_values, preferred_element_type...]
    reduce_scatter x1 -> x0, waiting for transfers between devices: 34.4 us -> none  [per_device(): lax.psum_scatter(jnp.dot(inner_rows, out_proj, preferred_element_type=jnp...]
    rev x10 -> x0, local copies, waits for them, and re-layouts: 30.1 us -> none  [the longest x1 9.38 us: per_device(): block_outputs(values[::-1], reads[::-1], backward_affinity, backward_cumu...]
    convert_element_type x12 -> x0, local copies, waits for them, and re-layouts: 20.8 us -> none  [the longest x5 9.56 us: convolve(): return jax.nn.silu(summed).reshape(length, channels).astype(jnp.bfloat16)]
    another operation x10 -> x0, other arithmetic: 11.9 us -> none
  transfers between devices with their start and end apart: 3 -> 0, of which waited for: 2 -> 0; matrix products, arithmetic and copies ran while one was open for 8% -> 0% of each run, Pallas kernels for 0% -> 0%
where the time goes in v1:
time: 132 us; the launch traced here: 131 us
  Pallas kernels  125 us (95%)
  local copies, waits for them, and re-layouts  4.51 us (3%)
  other arithmetic  1.4 us (1%)
    pallas_call x1, Pallas kernels, per_device(): call(functools.partial(spread_kernel, sp_n, tp_n), [shape((tokens, model)...  36.6 us
    pallas_call x1, Pallas kernels, per_device(): call(functools.partial(project_kernel, sp_n, heads, per_group), [shape((t...  27.3 us
    pallas_call x1, Pallas kernels, per_device(): call(functools.partial(finish_kernel, tp_n), shape((rows, model), BF16),...  25.3 us
    pallas_call x1, Pallas kernels, per_device(): call(functools.partial(states_kernel, sp_n, heads), shape((2, width, STAT...  23.4 us
    pallas_call x1, Pallas kernels, per_device(): call(functools.partial(sweep_kernel, heads, per_group), shape((tokens, mo...  12.7 us

profile of v1, /device:TPU:0, one launch (start us, length us, event | category | flops | bytes accessed | tf_op | source)
XLA Modules:
  0.0 131.3 jit_solution(15840343565221918421)
XLA Ops:
  0.0 0.0 copy-start
  0.0 0.8 fusion.7
  0.8 0.8 constant_dynamic-slice_fusion
  1.6 0.1 reshape.7
  1.6 0.6 pad.24.rates
  2.2 0.6 fusion.5.act
  2.8 0.0 copy-done
  2.9 0.3 copy.21
  3.1 0.9 pad.23.step_p
  4.0 36.6 %shard_map.181 = (bf16[512,2048]{1,0:T(8,128)(2,1)}, bf16[288,2048]{1,0:T(8,128)(2,1)}, f32[8,2048]{1,0:T(8,128)}) custom-call(bf16[48,128]{1,0:T(8,128)(2,1)} %fusion.5.act, bf16[128,2048]{1,0:T(8,128)(2,1)} %shift_m.1, bf16[128,2048]{1,0:T(8,128)(2,1)} %scale_m.1, bf16[128,2048]{1,0:T(8,128)(2,1)} %gate_m.1, bf16[128,2048]{1,0:T(8,128)(2,1)} %bitcast.9, ...), custom_call_target="tpu_custom_call" | custom-call | tf_op jit(solution)/shard_map/pallas_call | solution.py:487
  40.6 27.3 %shard_map.182 = (bf16[512,512]{1,0:T(8,128)(2,1)}, bf16[512,512]{1,0:T(8,128)(2,1)}, bf16[512,256]{1,0:T(8,128)(2,1)}, bf16[512,256]{1,0:T(8,128)(2,1)}, f32[51...) custom-call(bf16[512,2048]{1,0:T(8,128)(2,1)} %get-tuple-element.17., ...), custom_call_target="tpu_custom_call" | custom-call | tf_op jit(solution)/shard_map/pallas_call | solution.py:499
  67.9 23.4 %shard_map.183.starts = bf16[2,512,128]{2,1,0:T(8,128)(2,1)} custom-call(bf16[4,512,128]{2,1,0:T(8,128)(2,1)} %get-tuple-element.27.states, f32[32,128]{1,0:T(8,128)} %get-tuple-element.28.tots), custom_call_target="tpu_custom_call" | custom-call | tf_op jit(solution)/shard_map/pallas_call | solution.py:513
  91.3 12.7 %shard_map.184.mixed = bf16[512,2048]{1,0:T(8,128)(2,1)} custom-call(bf16[512,512]{1,0:T(8,128)(2,1)} %get-tuple-element.20.values, bf16[512,512]{1,0:T(8,128)(2,1)} %get-tuple-element.21.gate, bf16[512,256]{1,0:T(8,128)(2,1)} %get-tuple-element.22.writes, bf16[512,256]{1,0:T(8,128)(2,1)} %get-tuple-element.23.reads, f32[512,128]{1,0:T(8,128)} %get-tuple-element.24.step, ...), custom_call_target="tpu_custom_call" | custom-call | tf_op jit(solution)/shard_map/pallas_call | solution.py:523
  104.1 25.3 %shard_map.185 = bf16[128,2048]{1,0:T(8,128)(2,1)} custom-call(bf16[512,2048]{1,0:T(8,128)(2,1)} %shard_map.184.mixed, bf16[128,2048]{1,0:T(8,128)(2,1)} %bitcast.10, f32[8,2048]{1,0:T(8,128)} %get-tuple-element.19.mod), custom_call_target="tpu_custom_call" | custom-call | tf_op jit(solution)/shard_map/pallas_call | solution.py:531
  129.4 1.9 %copy.23 = bf16[1,128,2048]{2,1,0:T(8,128)(2,1)} copy(bf16[1,128,2048]{2,1,0:T(8,128)(2,1)} %bitcast.8) | data formatting | bytes 1048576
  (1 shorter events, 0.0 us)
Async XLA Ops:
  0.0 2.8 %copy-start = (bf16[2048,2,32]{0,2,1:T(8,128)(2,1)S(1)}, bf16[2048,2,32]{0,2,1:T(8,128)(2,1)}, u32[]{:S(2)}) copy-start(bf16[2048,2,32]{0,2,1:T(8,128)(2,1)} %param.30) | copy-start | bytes 786436

commit v2 on v1

v2 whole, which is shorter than its diff:
```python
import functools

import jax
import jax.numpy as jnp
from jax import lax
from jax.experimental import pallas as pl
from jax.experimental.pallas import tpu as pltpu
from jax.sharding import PartitionSpec as P

HEAD = 64
STATE = 128
ROW = 64
BLOCK = 128
LANES = 128
HALO = 16

NORM_FLOOR = 1e-05
GATED_FLOOR = 1e-06
FINEST = lax.Precision.HIGHEST
MESH = pl.DeviceIdType.MESH
F32 = jnp.float32
BF16 = jnp.bfloat16


def vmem():
    return pl.BlockSpec(memory_space=pltpu.VMEM)


def send(src, dst, send_sem, recv_sem, axis, target):
    copy = pltpu.make_async_remote_copy(
        src_ref=src,
        dst_ref=dst,
        send_sem=send_sem,
        recv_sem=recv_sem,
        device_id={axis: target},
        device_id_type=MESH,
    )
    copy.start()
    return copy


def greet(peers):
    barrier = pltpu.get_barrier_semaphore()
    for axis, target in peers:
        pl.semaphore_signal(barrier, inc=1, device_id={axis: target}, device_id_type=MESH)
    pl.semaphore_wait(barrier, len(peers))


def others(axis, count):
    me = lax.axis_index(axis)
    return [lax.rem(me + d, count) for d in range(1, count)]


def ring_of(place, count):
    def turn(p):
        high, low = lax.div(p, 2), lax.rem(p, 2)
        return high * 2 + lax.rem(high + low, 2)

    spot = turn(place)
    return [turn(lax.rem(spot + d, count)) for d in (1, 3, 2)]


def softplus(x):
    return jnp.maximum(x, 0.0) + jnp.log1p(jnp.exp(-jnp.abs(x)))


def silu(x):
    return x * (1.0 / (1.0 + jnp.exp(-x)))


def modulate_into(source, target, shift_row, scale_row):
    step = 16

    def tile(i, carry):
        at = pl.ds(pl.multiple_of(i * step, step), step)
        values = source[at, :].astype(F32)
        center = jnp.mean(values, -1, keepdims=True)
        values = values - center
        spread = jnp.mean(values * values, -1, keepdims=True)
        normed = values * lax.rsqrt(spread + NORM_FLOOR)
        target[at, :] = (normed * (1.0 + scale_row[...]) + shift_row[...]).astype(BF16)
        return carry

    lax.fori_loop(0, source.shape[0] // step, tile, 0)


def conv_silu(values, taps, run):
    rows, channels = values.shape
    margin = taps.shape[0] // 2
    place = lax.broadcasted_iota(jnp.int32, (rows, channels), 0) % run
    summed = jnp.zeros((rows, channels), F32)
    for k in range(taps.shape[0]):
        offset = k - margin
        moved = pltpu.roll(values, (-offset) % rows, 0) if offset else values
        if offset:
            moved = jnp.where((place + offset >= 0) & (place + offset < run), moved, 0.0)
        summed += moved * taps[k : k + 1, :]
    return silu(summed).astype(BF16)


def running(decay, heads):
    rows = decay.shape[0]
    at = lax.broadcasted_iota(jnp.int32, (rows, rows), 0)
    by = lax.broadcasted_iota(jnp.int32, (rows, rows), 1)
    lower = (by <= at).astype(F32)
    upper = (by >= at).astype(F32)
    lane = lax.broadcasted_iota(jnp.int32, decay.shape, 1)
    forward = jnp.dot(lower, decay, precision=FINEST, preferred_element_type=F32)
    backward = jnp.dot(upper, decay, precision=FINEST, preferred_element_type=F32)
    return jnp.where(lane < heads, forward, backward)


def lane_to_rows(row, count):
    return jnp.broadcast_to(row, (LANES, LANES)).T[0:count]


def partial_states(values, writes, weight, heads, per_group):
    turned = values.astype(F32).T.astype(BF16)
    result = []
    for h in range(heads):
        g = h // per_group
        rows = writes[:, g * STATE : (g + 1) * STATE].astype(F32)
        pair = jnp.concatenate(
            [(rows * weight[:, h : h + 1]).astype(BF16),
             (rows * weight[:, heads + h : heads + h + 1]).astype(BF16)], axis=1)
        result.append(
            jnp.dot(turned[h * HEAD : (h + 1) * HEAD], pair, preferred_element_type=F32))
    return result


def front_kernel(
    sp_n, tp_n, heads, per_group,
    act, shift_m, scale_m, gate_m, latent, context,
    value_h, gate_h, write_h, read_h, step_p, rates, pacing, value_t, write_t, read_t,
    values_o, gate_o, writes_o, reads_o, step_o, cumul_o, inc_o, ends_o, ctx_o, mod,
    value_p, gate_p, write_p, read_p,
    latent_all, context_ext, part, tp_box, middle, sp_box,
    hidden, hidden_c, ctx_v, ctx_w,
    c_states, c_tots, c_box, c_tot_box, c_out,
    own, lat_s, lat_r, tps, tpr, sps, spr, halo_s, halo_r, s1, r1, s2, r2, s3, r3,
):
    sp, tp = lax.axis_index("sp"), lax.axis_index("tp")
    tp_peers, sp_peers = others("tp", tp_n), others("sp", sp_n)
    rows, ctx_rows = latent.shape[0], context.shape[0]
    tokens, model = latent_all.shape
    ext = context_ext.shape[0]
    width, keys = value_p.shape[1], write_p.shape[1]
    blocks = tokens // BLOCK
    piece = 256
    loads = [
        pltpu.make_async_copy(src, dst, own.at[2 + i])
        for i, (src, dst) in enumerate(
            [(value_h, value_p), (write_h, write_p), (gate_h, gate_p), (read_h, read_p)])
    ]
    for copy in loads:
        copy.start()
    greet([("tp", p) for p in tp_peers] + [("sp", p) for p in sp_peers])

    def rows_at(p, count, start=0):
        return pl.ds(pl.multiple_of(p * rows + start, count), count)

    mine = rows_at(tp, rows)
    copy_lat = pltpu.make_async_copy(latent, latent_all.at[mine], own.at[0])
    copy_lat.start()
    copy_ctx = pltpu.make_async_copy(context, context_ext.at[pl.ds(HALO, ctx_rows)], own.at[1])
    copy_ctx.start()
    before = lax.rem(sp + sp_n - 1, sp_n)
    after = lax.rem(sp + 1, sp_n)
    halos = [
        send(context.at[pl.ds(ctx_rows - HALO, HALO)], context_ext.at[pl.ds(0, HALO)],
             halo_s.at[0], halo_r.at[0], "sp", after),
        send(context.at[pl.ds(0, HALO)], context_ext.at[pl.ds(HALO + ctx_rows, HALO)],
             halo_s.at[1], halo_r.at[1], "sp", before),
    ]
    total = jnp.dot(act[0:16, :], shift_m[...], preferred_element_type=F32)
    total += jnp.dot(act[16:32, :], scale_m[...], preferred_element_type=F32)
    total += jnp.dot(act[32:48, :], gate_m[...], preferred_element_type=F32)
    for c in range(model // LANES):
        part[5 * c : 5 * c + 5, :] = total[0:5, c * LANES : (c + 1) * LANES]
    first = [
        send(part, tp_box.at[d], tps.at[d], tpr.at[d], "tp", p) for d, p in enumerate(tp_peers)
    ]
    if tp_n == 4:
        right, left, opposite = ring_of(tp, tp_n)
        to_right = send(latent, latent_all.at[mine], lat_s.at[0], lat_r.at[0], "tp", right)
        to_left = send(latent, latent_all.at[mine], lat_s.at[1], lat_r.at[1], "tp", left)
        moves = [to_right, to_left]
    else:
        moves = [
            send(latent, latent_all.at[mine], lat_s.at[d], lat_r.at[d], "tp", p)
            for d, p in enumerate(tp_peers)
        ]
    for copy in first:
        copy.wait()
    summed = part[...]
    for d in range(tp_n - 1):
        summed += tp_box[d]
    middle[...] = summed
    second = [
        send(middle, sp_box.at[d], sps.at[d], spr.at[d], "sp", p) for d, p in enumerate(sp_peers)
    ]
    for copy in second:
        copy.wait()
    summed = middle[...]
    for d in range(sp_n - 1):
        summed += sp_box[d]
    middle[...] = summed
    mod[...] = jnp.zeros_like(mod)
    for c in range(model // LANES):
        mod[0:5, c * LANES : (c + 1) * LANES] = middle[5 * c : 5 * c + 5, :]
    for copy in halos:
        copy.wait()
    copy_lat.wait()
    copy_ctx.wait()
    if tp_n == 4:
        half = rows // 2
        to_right.wait()
        on_right = send(latent_all.at[rows_at(left, half)], latent_all.at[rows_at(left, half)],
                        lat_s.at[2], lat_r.at[2], "tp", right)
        to_left.wait()
        on_left = send(latent_all.at[rows_at(right, half, half)],
                       latent_all.at[rows_at(right, half, half)],
                       lat_s.at[3], lat_r.at[3], "tp", left)
        moves = [on_right, on_left]

    modulate_into(context_ext, hidden_c, mod.at[1:2, :], mod.at[3:4, :])

    def taps_at(ref, start):
        return ref[:, pl.ds(pl.multiple_of(start, piece), piece)]

    place = lax.broadcasted_iota(jnp.int32, (ext, piece), 0)
    live = ((place >= HALO) | (sp > 0)) & ((place < HALO + ctx_rows) | (sp < sp_n - 1))

    def latent_part(weight, taps, total, out):
        for c in range(0, total, piece):
            pre = jnp.dot(hidden[...], weight[:, c : c + piece], preferred_element_type=F32)
            pre = pre.astype(BF16)
            if taps is None:
                out[:, c : c + piece] = pre
            else:
                kernel = taps_at(taps, tp * total + c)
                out[:, c : c + piece] = conv_silu(pre.astype(F32), kernel, ROW)

    def context_part(weight, taps, total, out):
        for c in range(0, total, piece):
            pre = jnp.dot(hidden_c[...], weight[:, c : c + piece], preferred_element_type=F32)
            pre = jnp.where(live, pre.astype(BF16).astype(F32), 0.0)
            done = conv_silu(pre, taps_at(taps, tp * total + c), ext)
            out[:, c : c + piece] = done[HALO : HALO + ctx_rows]

    rate = rates[0:1, :]
    loads[0].wait()
    loads[1].wait()
    context_part(value_p, value_t, width, ctx_v)
    context_part(write_p, write_t, keys, ctx_w)
    raw_c = jnp.dot(hidden_c[...], step_p[...], preferred_element_type=F32).astype(BF16)
    step_c = softplus(raw_c.astype(F32))[HALO : HALO + ctx_rows]
    decay_c = -rate * step_c
    total_c = jnp.sum(decay_c, axis=0, keepdims=True)
    weight_c = jnp.exp(total_c - running(decay_c, heads)) * step_c
    found = partial_states(ctx_v[...], ctx_w[...], weight_c, heads, per_group)
    for h in range(heads):
        at = slice(h * HEAD, (h + 1) * HEAD)
        c_states[0, at, :] = found[h][:, 0:STATE].astype(BF16)
        c_states[1, at, :] = found[h][:, STATE : 2 * STATE].astype(BF16)
    c_tots[...] = lane_to_rows(total_c, 2 * heads)

    share = width // sp_n

    def share_of(p):
        return pl.ds(pl.multiple_of(p * share, share), share)

    gathers = []
    for d, p in enumerate(sp_peers):
        gathers.append(send(c_tots, c_tot_box.at[sp], s2.at[d], r2.at[d], "sp", p))
        gathers.append(
            send(c_states.at[:, share_of(p), :], c_box.at[sp], s1.at[d], r1.at[d], "sp", p))
    c_box[sp] = c_states[:, share_of(sp), :]
    c_tot_box[sp] = c_tots[...]

    for copy in moves:
        copy.wait()
    modulate_into(latent_all, hidden, mod.at[0:1, :], mod.at[2:3, :])

    for copy in gathers:
        copy.wait()
    head_at = (sp * share) // HEAD
    each = min(HEAD, share)

    def factor(j, base):
        found = [
            jnp.broadcast_to(
                jnp.exp(c_tot_box[j, pl.ds(base + head_at + q, 1), :]), (each, STATE))
            for q in range(max(1, share // HEAD))
        ]
        return found[0] if len(found) == 1 else jnp.concatenate(found, axis=0)

    forward = jnp.zeros((share, STATE), F32)
    for j in range(sp_n):
        forward = factor(j, 0) * forward + c_box[j, 0].astype(F32)
    backward = jnp.zeros((share, STATE), F32)
    for j in range(sp_n - 1, -1, -1):
        backward = factor(j, heads) * backward + c_box[j, 1].astype(F32)
    c_out[0] = forward.astype(BF16)
    c_out[1] = backward.astype(BF16)
    back = [
        send(c_out, ctx_o.at[:, share_of(sp), :], s3.at[d], r3.at[d], "sp", p)
        for d, p in enumerate(sp_peers)
    ]
    ctx_o[:, share_of(sp), :] = c_out[...]

    latent_part(value_p, value_t, width, values_o)
    latent_part(write_p, write_t, keys, writes_o)
    loads[2].wait()
    loads[3].wait()
    latent_part(gate_p, None, width, gate_o)
    latent_part(read_p, read_t, keys, reads_o)
    raw = jnp.dot(hidden[...], step_p[...], preferred_element_type=F32).astype(BF16)
    pace = pacing[:, pl.ds(pl.multiple_of(sp * tokens, tokens), tokens)]
    pace = jnp.broadcast_to(pace, (LANES, tokens)).T
    step_o[...] = softplus(raw.astype(F32)) * pace
    drops = []
    for k in range(blocks):
        at = slice(k * BLOCK, (k + 1) * BLOCK)
        step = step_o[at, :]
        decay = -rate * step
        cumul = running(decay, heads)
        total = jnp.sum(decay, axis=0, keepdims=True)
        cumul_o[at, :] = cumul
        weight = jnp.exp(total - cumul) * step
        drops.append(jnp.exp(total))
        found = partial_states(values_o[at, :], writes_o[at, :], weight, heads, per_group)
        for h in range(heads):
            inc_o[k, h * HEAD : (h + 1) * HEAD, :] = found[h]
    for h in range(heads):
        at = slice(h * HEAD, (h + 1) * HEAD)
        forward = inc_o[0, at, 0:STATE]
        for k in range(1, blocks):
            forward = drops[k][:, h : h + 1] * forward + inc_o[k, at, 0:STATE]
        backward = inc_o[blocks - 1, at, STATE : 2 * STATE]
        for k in range(blocks - 2, -1, -1):
            backward = (
                drops[k][:, heads + h : heads + h + 1] * backward
                + inc_o[k, at, STATE : 2 * STATE])
        ends_o[0, at, :] = forward
        ends_o[1, at, :] = backward
    for copy in back:
        copy.wait()


def sweep_kernel(
    sp_n, heads, per_group,
    values, gate, writes, reads, step, cumul, inc, ends, ctx, gain,
    inner,
    starts, outgoing, state_f, state_b, joined, ss, rs,
):
    sp, tp = lax.axis_index("sp"), lax.axis_index("tp")
    tokens, width = values.shape
    blocks = tokens // BLOCK
    span = per_group * HEAD
    groups = heads // per_group
    after, before = lax.rem(sp + 1, sp_n), lax.rem(sp + sp_n - 1, sp_n)
    greet([("sp", after), ("sp", before)])
    lane = lax.broadcasted_iota(jnp.int32, (1, LANES), 1)
    totals = [
        jnp.where(
            lane < heads,
            cumul[(k + 1) * BLOCK - 1 : (k + 1) * BLOCK, :],
            cumul[k * BLOCK : k * BLOCK + 1, :])
        for k in range(blocks)
    ]
    drops = [jnp.exp(t) for t in totals]
    grand = totals[0]
    for t in totals[1:]:
        grand = grand + t
    grand = jnp.exp(grand)
    chunk = 2 * HEAD
    chunks = width // chunk

    def link(way, c):
        at = pl.ds(c * chunk, chunk)
        return pltpu.make_async_remote_copy(
            src_ref=outgoing.at[way, at],
            dst_ref=starts.at[way, at],
            send_sem=ss.at[way * chunks + c],
            recv_sem=rs.at[way * chunks + c],
            device_id={"sp": before if way else after},
            device_id_type=MESH,
        )

    def chain(way):
        enters = sp == (sp_n - 1 if way else 0)
        leaves = sp == (0 if way else sp_n - 1)

        @pl.when(enters)
        def _():
            starts[way] = ctx[way]

        for c in range(chunks):
            @pl.when(jnp.logical_not(enters))
            def _():
                link(way, c).wait_recv()

            @pl.when(jnp.logical_not(leaves))
            def _():
                for q in range(chunk // HEAD):
                    h = c * (chunk // HEAD) + q
                    at = slice(h * HEAD, (h + 1) * HEAD)
                    j = way * heads + h
                    outgoing[way, at, :] = (
                        grand[:, j : j + 1] * starts[way, at, :].astype(F32) + ends[way, at, :]
                    ).astype(BF16)
                link(way, c).start()

    at_row = lax.broadcasted_iota(jnp.int32, (BLOCK, BLOCK), 0)
    by_row = lax.broadcasted_iota(jnp.int32, (BLOCK, BLOCK), 1)
    past, diagonal = by_row <= at_row, by_row == at_row
    contract = (((1,), (1,)), ((), ()))

    def local_block(k):
        rows = slice(k * BLOCK, (k + 1) * BLOCK)
        c = cumul[rows, :]
        c_turned, s_turned = c.T, step[rows, :].T
        for g in range(groups):
            keys = slice(g * STATE, (g + 1) * STATE)
            affinity = lax.dot_general(
                reads[rows, keys], writes[rows, keys], contract, preferred_element_type=F32)
            for r in range(per_group):
                h = g * per_group + r
                b = heads + h
                head = slice(h * HEAD, (h + 1) * HEAD)
                exponent = jnp.where(
                    past,
                    c[:, h : h + 1] - c_turned[h : h + 1, :],
                    c[:, b : b + 1] - c_turned[b : b + 1, :])
                fs, bs = s_turned[h : h + 1, :], s_turned[b : b + 1, :]
                steps = jnp.where(past, fs, bs) + jnp.where(diagonal, bs, 0.0)
                mixing = (affinity * jnp.exp(exponent) * steps).astype(BF16)
                joined[rows, head] = jnp.dot(
                    mixing, values[rows, head], preferred_element_type=F32)

    for slot in range(blocks):
        last = slot == blocks - 1
        for way in range(2):
            turn = (sp_n - 1 - sp) if way else sp
            pl.when(turn >= slot if last else turn == slot)(functools.partial(chain, way))
        local_block(slot)

    for way in range(2):
        @pl.when(sp != (0 if way else sp_n - 1))
        def _():
            for c in range(chunks):
                link(way, c).wait_send()

    for h in range(heads):
        rows = slice(h * HEAD, (h + 1) * HEAD)
        forward = starts[0, rows, :].astype(F32)
        for k in range(blocks):
            state_f[k, rows, :] = forward.astype(BF16)
            forward = drops[k][:, h : h + 1] * forward + inc[k, rows, 0:STATE]
        backward = starts[1, rows, :].astype(F32)
        for k in range(blocks - 1, -1, -1):
            state_b[k, rows, :] = backward.astype(BF16)
            backward = (
                drops[k][:, heads + h : heads + h + 1] * backward
                + inc[k, rows, STATE : 2 * STATE])

    def carried_block(k, carry):
        rows = pl.ds(pl.multiple_of(k * BLOCK, BLOCK), BLOCK)
        grown = jnp.exp(cumul[rows, :])
        for g in range(groups):
            read = reads[rows, g * STATE : (g + 1) * STATE].astype(F32)
            for r in range(per_group):
                h = g * per_group + r
                b = heads + h
                head = slice(h * HEAD, (h + 1) * HEAD)
                left = jnp.concatenate(
                    [(read * grown[:, h : h + 1]).astype(BF16),
                     (read * grown[:, b : b + 1]).astype(BF16)], axis=1)
                right = jnp.concatenate([state_f[k, head, :], state_b[k, head, :]], axis=1)
                joined[rows, head] += lax.dot_general(
                    left, right, contract, preferred_element_type=F32)
            lanes = slice(g * span, (g + 1) * span)
            gated = joined[rows, lanes] * silu(gate[rows, lanes].astype(F32))
            scale = lax.rsqrt(jnp.mean(gated * gated, -1, keepdims=True) + GATED_FLOOR)
            start = pl.multiple_of(tp * width + g * span, span)
            inner[rows, lanes] = (gated * scale * gain[:, pl.ds(start, span)]).astype(BF16)
        return carry

    lax.fori_loop(0, blocks, carried_block, 0)


def finish_kernel(tp_n, inner, out_p, total_o, mixed, early, relay, box, ss, rs):
    tp = lax.axis_index("tp")
    peers = others("tp", tp_n)
    rows, model = total_o.shape
    greet([("tp", p) for p in peers])

    def product(owner):
        at = pl.ds(pl.multiple_of(owner * rows, rows), rows)
        for c in range(0, model, 512):
            mixed[at, c : c + 512] = jnp.dot(
                inner[at, :], out_p[:, c : c + 512], preferred_element_type=F32).astype(BF16)

    def rows_at(p, count, start=0):
        return pl.ds(pl.multiple_of(p * rows + start, count), count)

    if tp_n == 4:
        half = rows // 2
        low, high = pl.ds(0, half), pl.ds(half, half)
        right, left, opposite = ring_of(tp, tp_n)
        product(opposite)
        far = [
            send(mixed.at[rows_at(opposite, half)], early.at[0], ss.at[0], rs.at[0], "tp", right),
            send(mixed.at[rows_at(opposite, half, half)], early.at[1],
                 ss.at[1], rs.at[1], "tp", left),
        ]
        product(right)
        copies = [send(mixed.at[rows_at(right, half, half)], box.at[0, high],
                       ss.at[2], rs.at[2], "tp", right)]
        product(left)
        copies.append(send(mixed.at[rows_at(left, half)], box.at[1, low],
                           ss.at[3], rs.at[3], "tp", left))
        product(tp)
        for way, (owner, start, lands) in enumerate([(right, 0, low), (left, half, high)]):
            far[way].wait()
            relay[way] = (
                mixed[rows_at(owner, half, start), :].astype(F32) + early[way].astype(F32)
            ).astype(BF16)
            copies.append(send(relay.at[way], box.at[way, lands],
                               ss.at[4 + way], rs.at[4 + way], "tp", owner))
        landed = 2
    else:
        for p in peers + [tp]:
            product(p)
        copies = [
            send(mixed.at[rows_at(p, rows)], box.at[d], ss.at[d], rs.at[d], "tp", p)
            for d, p in enumerate(peers)
        ]
        landed = tp_n - 1
    for copy in copies:
        copy.wait()
    tile_rows = 16

    def tile(i, carry):
        at = pl.ds(pl.multiple_of(i * tile_rows, tile_rows), tile_rows)
        own = pl.ds(pl.multiple_of(tp * rows + i * tile_rows, tile_rows), tile_rows)
        total = mixed[own, :].astype(F32)
        for d in range(landed):
            total += box[d, at, :].astype(F32)
        total_o[at, :] = total.astype(BF16)
        return carry

    lax.fori_loop(0, rows // tile_rows, tile, 0)


def shape(dims, kind):
    return jax.ShapeDtypeStruct(dims, kind)


def call(body, outs, specs, scratch, collective, limit=60 << 20):
    params = dict(vmem_limit_bytes=limit, collective_id=collective, has_side_effects=True)
    single = not isinstance(outs, (list, tuple))
    return pl.pallas_call(
        body,
        out_shape=outs,
        in_specs=specs,
        out_specs=vmem() if single else [vmem()] * len(outs),
        scratch_shapes=scratch,
        compiler_params=pltpu.CompilerParams(**params),
    )


def dma(count):
    return pltpu.SemaphoreType.DMA((count,))


def per_device(
    sp_n, tp_n,
    latent, condition, context, context_cond, shift_matrix, scale_matrix, gate_matrix,
    value_proj, gate_proj, write_proj, read_proj, step_proj, decay_rate, pacing,
    value_taps, write_taps, read_taps, norm_gain, out_proj,
):
    sp, tp = lax.axis_index("sp"), lax.axis_index("tp")
    rows, model = latent.shape[1:]
    ctx_rows = context.shape[1]
    tokens = rows * tp_n
    width, keys = value_proj.shape[1], write_proj.shape[1]
    heads = width // HEAD
    per_group = heads // (keys // STATE)
    blocks = tokens // BLOCK
    row_share = shift_matrix.shape[0]

    pair = jnp.stack([condition[0], context_cond])
    pair = lax.dynamic_slice_in_dim(pair, (sp * tp_n + tp) * row_share, row_share, 1)
    pair = jax.nn.silu(pair).astype(BF16)
    act = jnp.concatenate([
        jnp.pad(pair, ((0, 14), (0, 0))),
        jnp.pad(pair, ((2, 12), (0, 0))),
        jnp.pad(pair[:1], ((4, 11), (0, 0))),
    ])
    step_cols = lax.dynamic_slice_in_dim(step_proj, tp * heads, heads, 2)
    step_cols = jnp.pad(step_cols.reshape(model, 2 * heads), ((0, 0), (0, LANES - 2 * heads)))
    rates = lax.dynamic_slice_in_dim(decay_rate, tp * heads, heads, 1).reshape(1, 2 * heads)
    rates = jnp.pad(rates, ((0, 7), (0, LANES - 2 * heads)))

    held = pl.BlockSpec(memory_space=pl.ANY)
    ext = ctx_rows + 2 * HALO
    share = width // sp_n
    packed = 5 * model // LANES
    values, gate, writes, reads, step, cumul, inc, ends, ctx, mod = call(
        functools.partial(front_kernel, sp_n, tp_n, heads, per_group),
        [shape((tokens, width), BF16), shape((tokens, width), BF16),
         shape((tokens, keys), BF16), shape((tokens, keys), BF16),
         shape((tokens, LANES), F32), shape((tokens, LANES), F32),
         shape((blocks, width, 2 * STATE), F32), shape((2, width, STATE), F32),
         shape((2, width, STATE), BF16), shape((8, model), F32)],
        [vmem()] * 6 + [held] * 4 + [vmem()] * 6,
        [pltpu.VMEM((model, width), BF16), pltpu.VMEM((model, width), BF16),
         pltpu.VMEM((model, keys), BF16), pltpu.VMEM((model, keys), BF16),
         pltpu.VMEM((tokens, model), BF16), pltpu.VMEM((ext, model), BF16),
         pltpu.VMEM((packed, LANES), F32), pltpu.VMEM((tp_n - 1, packed, LANES), F32),
         pltpu.VMEM((packed, LANES), F32), pltpu.VMEM((sp_n - 1, packed, LANES), F32),
         pltpu.VMEM((tokens, model), BF16), pltpu.VMEM((ext, model), BF16),
         pltpu.VMEM((ctx_rows, width), BF16), pltpu.VMEM((ctx_rows, keys), BF16),
         pltpu.VMEM((2, width, STATE), BF16), pltpu.VMEM((2 * heads, LANES), F32),
         pltpu.VMEM((sp_n, 2, share, STATE), BF16), pltpu.VMEM((sp_n, 2 * heads, LANES), F32),
         pltpu.VMEM((2, share, STATE), BF16),
         dma(6), dma(tp_n), dma(tp_n), dma(tp_n), dma(tp_n), dma(sp_n), dma(sp_n), dma(2), dma(2),
         dma(sp_n), dma(sp_n), dma(sp_n), dma(sp_n), dma(sp_n), dma(sp_n)],
        0,
    )(act, shift_matrix, scale_matrix, gate_matrix, latent[0], context[0],
      value_proj, gate_proj, write_proj, read_proj, step_cols,
      rates, pacing, value_taps, write_taps, read_taps)

    pieces = 2 * (width // (2 * HEAD))
    inner = call(
        functools.partial(sweep_kernel, sp_n, heads, per_group),
        shape((tokens, width), BF16),
        [vmem()] * 10,
        [pltpu.VMEM((2, width, STATE), BF16), pltpu.VMEM((2, width, STATE), BF16),
         pltpu.VMEM((blocks, width, STATE), BF16), pltpu.VMEM((blocks, width, STATE), BF16),
         pltpu.VMEM((tokens, width), F32), dma(pieces), dma(pieces)],
        1,
    )(values, gate, writes, reads, step, cumul, inc, ends, ctx, norm_gain[None])

    total = call(
        functools.partial(finish_kernel, tp_n),
        shape((rows, model), BF16),
        [vmem()] * 2,
        [pltpu.VMEM((tokens, model), BF16), pltpu.VMEM((2, rows // 2, model), BF16),
         pltpu.VMEM((2, rows // 2, model), BF16), pltpu.VMEM((tp_n - 1, rows, model), BF16),
         dma(6), dma(6)],
        2,
    )(inner, out_proj)
    updated = latent[0].astype(F32) + mod[4:5] * lax.optimization_barrier(total).astype(F32)
    return updated.astype(BF16)[None]


def solution(mesh):
    placed = (
        P("dp", ("sp", "tp"), None),
        P("dp", None),
        P("dp", "sp", None),
        P(),
        P(("sp", "tp"), None),
        P(("sp", "tp"), None),
        P(("sp", "tp"), None),
        P(None, "tp"),
        P(None, "tp"),
        P(None, "tp"),
        P(None, "tp"),
        P(),
        P(),
        P("dp", None),
        P(),
        P(),
        P(),
        P(),
        P("tp", None),
    )
    return jax.shard_map(
        functools.partial(per_device, mesh.shape["sp"], mesh.shape["tp"]),
        mesh=mesh,
        in_specs=placed,
        out_specs=P("dp", ("sp", "tp"), None),
        check_vma=False,
    )
```

time: 132 us -> 97.6 us (0.74)
  Pallas kernels: 125 us -> 90.4 us
  other arithmetic: 1.4 us -> 3.39 us
    pallas_call x4 -> x2, Pallas kernels: 100 us -> 69.8 us  [the longest x1 49.2 us: per_device(): call(functools.partial(front_kernel, sp_n, tp_n, heads, per_group), [shap...]
    pallas_call x1, Pallas kernels: 25.3 us -> 20.6 us  [per_device(): call(functools.partial(finish_kernel, tp_n), shape((rows, model), BF16),...]
    broadcast_in_dim x0 -> x1, other arithmetic: none -> 2 us  [per_device(): return updated.astype(BF16)[None]]
    unnamed x3 -> x4, local copies, waits for them, and re-layouts: 1.89 us -> 0.01 us
where the time goes in v2:
time: 97.6 us; the launch traced here: 97.3 us
  Pallas kernels  90.4 us (93%)
  local copies, waits for them, and re-layouts  3.48 us (4%)
  other arithmetic  3.39 us (3%)
    pallas_call x1, Pallas kernels, per_device(): call(functools.partial(front_kernel, sp_n, tp_n, heads, per_group), [shap...  49.2 us
    pallas_call x1, Pallas kernels, per_device(): call(functools.partial(finish_kernel, tp_n), shape((rows, model), BF16),...  20.6 us
    pallas_call x1, Pallas kernels, per_device(): call(functools.partial(sweep_kernel, sp_n, heads, per_group), shape((toke...  20.6 us
    broadcast_in_dim x1, other arithmetic, per_device(): return updated.astype(BF16)[None]  2 us

profile of v2, /device:TPU:0, one launch (start us, length us, event | category | flops | bytes accessed | tf_op | source)
XLA Modules:
  0.0 97.3 jit_solution(13047197466153511738)
XLA Ops:
  0.0 0.0 copy-start
  0.0 0.8 fusion.8
  0.8 0.8 constant_dynamic-slice_fusion
  1.6 0.1 reshape.7
  1.6 0.6 pad.24.rates
  2.2 0.6 fusion.6.act
  2.8 0.0 copy-done
  2.9 0.3 copy.21
  3.1 0.9 pad.23.step_p
  4.0 49.2 %shard_map.181 = (bf16[512,512]{1,0:T(8,128)(2,1)}, bf16[512,512]{1,0:T(8,128)(2,1)}, bf16[512,256]{1,0:T(8,128)(2,1)}, bf16[512,256]{1,0:T(8,128)(2,1)}, f32[51...) custom-call(bf16[48,128]{1,0:T(8,128)(2,1)} %fusion.6.act, ...), custom_call_target="tpu_custom_call" | custom-call | tf_op jit(solution)/shard_map/pallas_call | solution.py:611
  53.3 0.8 slice.7
  54.1 20.6 %shard_map.182.inner = bf16[512,512]{1,0:T(8,128)(2,1)} custom-call(bf16[512,512]{1,0:T(8,128)(2,1)} %get-tuple-element.16.values, bf16[512,512]{1,0:T(8,128)(2,1)} %get-tuple-element.17.gate, bf16[512,256]{1,0:T(8,128)(2,1)} %get-tuple-element.18.writes, bf16[512,256]{1,0:T(8,128)(2,1)} %get-tuple-element.19.reads, f32[512,128]{1,0:T(8,128)} %get-tuple-element.20.step, ...), custom_call_target="tpu_custom_call" | custom-call | tf_op jit(solution)/shard_map/pallas_call | solution.py:637
  74.7 0.0 copy-start.1
  74.7 20.6 %shard_map.183 = bf16[128,2048]{1,0:T(8,128)(2,1)} custom-call(bf16[512,512]{1,0:T(8,128)(2,1)} %shard_map.182.inner, bf16[512,2048]{1,0:T(8,128)(2,1)} %out_p.1), custom_call_target="tpu_custom_call" | custom-call | tf_op jit(solution)/shard_map/pallas_call | solution.py:647
  95.3 0.0 copy-done.1
  95.3 2.0 %fusion = bf16[1,128,2048]{2,1,0:T(8,128)(2,1)} fusion(bf16[128,2048]{1,0:T(8,128)(2,1)} %shard_map.183, f32[2048]{0:T(1024)S(1)} %bitcast.13, bf16[1,128,2048]{2,1,0:T(8,128)(2,1)S(1)} %copy-done.1), kind=kLoop, calls=%fused_computation.1 | loop fusion | flops 1310720 | bytes 1581056 | tf_op jit(solution)/shard_map/broadcast_in_dim | solution.py:657
  (1 shorter events, 0.0 us)
Async XLA Ops:
  0.0 2.8 %copy-start = (bf16[2048,2,32]{0,2,1:T(8,128)(2,1)S(1)}, bf16[2048,2,32]{0,2,1:T(8,128)(2,1)}, u32[]{:S(2)}) copy-start(bf16[2048,2,32]{0,2,1:T(8,128)(2,1)} %param.30) | copy-start | bytes 786436
  74.7 20.6 %copy-start.1 = (bf16[1,128,2048]{2,1,0:T(8,128)(2,1)S(1)}, bf16[1,128,2048]{2,1,0:T(8,128)(2,1)}, u32[]{:S(2)}) copy-start(bf16[1,128,2048]{2,1,0:T(8,128)(2,1)} %param.19) | copy-start | bytes 1572868

commit v3 on v2

--- a/solution.py
+++ b/solution.py
@@ -13,6 +13,7 @@
 BLOCK = 128
 LANES = 128
 HALO = 16
+FRONT = 34
 
 NORM_FLOOR = 1e-05
 GATED_FLOOR = 1e-06
@@ -182,9 +183,16 @@
     ]
     if tp_n == 4:
         right, left, opposite = ring_of(tp, tp_n)
-        to_right = send(latent, latent_all.at[mine], lat_s.at[0], lat_r.at[0], "tp", right)
-        to_left = send(latent, latent_all.at[mine], lat_s.at[1], lat_r.at[1], "tp", left)
-        moves = [to_right, to_left]
+        half = rows // 2
+
+        def pass_on(owner, start, target, i):
+            at = rows_at(owner, half, start)
+            src = latent.at[pl.ds(start, half)] if owner is tp else latent_all.at[at]
+            return send(src, latent_all.at[at], lat_s.at[i], lat_r.at[i], "tp", target)
+
+        to_right = pass_on(tp, 0, right, 0)
+        to_left = pass_on(tp, half, left, 1)
+        moves = [pass_on(tp, half, right, 2), pass_on(tp, 0, left, 3)]
     else:
         moves = [
             send(latent, latent_all.at[mine], lat_s.at[d], lat_r.at[d], "tp", p)
@@ -213,15 +221,10 @@
     copy_lat.wait()
     copy_ctx.wait()
     if tp_n == 4:
-        half = rows // 2
         to_right.wait()
-        on_right = send(latent_all.at[rows_at(left, half)], latent_all.at[rows_at(left, half)],
-                        lat_s.at[2], lat_r.at[2], "tp", right)
+        moves.append(pass_on(left, 0, right, 4))
         to_left.wait()
-        on_left = send(latent_all.at[rows_at(right, half, half)],
-                       latent_all.at[rows_at(right, half, half)],
-                       lat_s.at[3], lat_r.at[3], "tp", left)
-        moves = [on_right, on_left]
+        moves.append(pass_on(right, half, left, 5))
 
     modulate_into(context_ext, hidden_c, mod.at[1:2, :], mod.at[3:4, :])
 
@@ -248,7 +251,13 @@
             done = conv_silu(pre, taps_at(taps, tp * total + c), ext)
             out[:, c : c + piece] = done[HALO : HALO + ctx_rows]
 
-    rate = rates[0:1, :]
+    pick_i = lax.broadcasted_iota(jnp.int32, (rates.shape[1], LANES), 0)
+    pick_l = lax.broadcasted_iota(jnp.int32, (rates.shape[1], LANES), 1)
+    pick = (pick_i == tp * heads + lax.rem(pick_l, heads)).astype(F32)
+    chosen = jnp.dot(rates[...], pick, precision=FINEST, preferred_element_type=F32)
+    lane_at = lax.broadcasted_iota(jnp.int32, (1, LANES), 1)
+    rate = jnp.where(
+        lane_at < heads, chosen[0:1, :], jnp.where(lane_at < 2 * heads, chosen[1:2, :], 0.0))
     loads[0].wait()
     loads[1].wait()
     context_part(value_p, value_t, width, ctx_v)
@@ -360,7 +369,6 @@
     span = per_group * HEAD
     groups = heads // per_group
     after, before = lax.rem(sp + 1, sp_n), lax.rem(sp + sp_n - 1, sp_n)
-    greet([("sp", after), ("sp", before)])
     lane = lax.broadcasted_iota(jnp.int32, (1, LANES), 1)
     totals = [
         jnp.where(
@@ -494,7 +502,6 @@
     tp = lax.axis_index("tp")
     peers = others("tp", tp_n)
     rows, model = total_o.shape
-    greet([("tp", p) for p in peers])
 
     def product(owner):
         at = pl.ds(pl.multiple_of(owner * rows, rows), rows)
@@ -554,6 +561,23 @@
     lax.fori_loop(0, rows // tile_rows, tile, 0)
 
 
+def whole_kernel(sp_n, tp_n, heads, per_group, *refs):
+    front_in, (gain, out_h) = refs[:16], refs[16:18]
+    total_o, gate_row_o = refs[18:20]
+    made, refs = refs[20:30], refs[30:]
+    front, refs = refs[:FRONT], refs[FRONT:]
+    sweep, refs = refs[:7], refs[7:]
+    inner, out_p, out_sem = refs[:3]
+    load = pltpu.make_async_copy(out_h, out_p, out_sem.at[0])
+    load.start()
+    front_kernel(sp_n, tp_n, heads, per_group, *front_in, *made, *front)
+    values, gate, writes, reads, step, cumul, inc, ends, ctx, mod = made
+    gate_row_o[...] = mod[4:5, :]
+    sweep_kernel(sp_n, heads, per_group, *made[:9], gain, inner, *sweep)
+    load.wait()
+    finish_kernel(tp_n, inner, out_p, total_o, *refs[3:])
+
+
 def shape(dims, kind):
     return jax.ShapeDtypeStruct(dims, kind)
 
@@ -591,69 +615,65 @@
     blocks = tokens // BLOCK
     row_share = shift_matrix.shape[0]
 
-    pair = jnp.stack([condition[0], context_cond])
-    pair = lax.dynamic_slice_in_dim(pair, (sp * tp_n + tp) * row_share, row_share, 1)
-    pair = jax.nn.silu(pair).astype(BF16)
-    act = jnp.concatenate([
-        jnp.pad(pair, ((0, 14), (0, 0))),
-        jnp.pad(pair, ((2, 12), (0, 0))),
-        jnp.pad(pair[:1], ((4, 11), (0, 0))),
-    ])
+    start = (sp * tp_n + tp) * row_share
+    own_row = lax.dynamic_slice_in_dim(condition, start, row_share, 1)
+    ctx_row = lax.dynamic_slice_in_dim(context_cond, start, row_share, 0)[None]
+    at = lax.broadcasted_iota(jnp.int32, (48, row_share), 0)
+    is_own = (at == 0) | (at == 18) | (at == 36)
+    is_ctx = (at == 1) | (at == 19)
+    act = jnp.where(is_own, own_row, jnp.where(is_ctx, ctx_row, 0.0))
+    act = jax.nn.silu(act).astype(BF16)
     step_cols = lax.dynamic_slice_in_dim(step_proj, tp * heads, heads, 2)
     step_cols = jnp.pad(step_cols.reshape(model, 2 * heads), ((0, 0), (0, LANES - 2 * heads)))
-    rates = lax.dynamic_slice_in_dim(decay_rate, tp * heads, heads, 1).reshape(1, 2 * heads)
-    rates = jnp.pad(rates, ((0, 7), (0, LANES - 2 * heads)))
-
     held = pl.BlockSpec(memory_space=pl.ANY)
     ext = ctx_rows + 2 * HALO
     share = width // sp_n
     packed = 5 * model // LANES
-    values, gate, writes, reads, step, cumul, inc, ends, ctx, mod = call(
-        functools.partial(front_kernel, sp_n, tp_n, heads, per_group),
-        [shape((tokens, width), BF16), shape((tokens, width), BF16),
-         shape((tokens, keys), BF16), shape((tokens, keys), BF16),
-         shape((tokens, LANES), F32), shape((tokens, LANES), F32),
-         shape((blocks, width, 2 * STATE), F32), shape((2, width, STATE), F32),
-         shape((2, width, STATE), BF16), shape((8, model), F32)],
-        [vmem()] * 6 + [held] * 4 + [vmem()] * 6,
-        [pltpu.VMEM((model, width), BF16), pltpu.VMEM((model, width), BF16),
-         pltpu.VMEM((model, keys), BF16), pltpu.VMEM((model, keys), BF16),
-         pltpu.VMEM((tokens, model), BF16), pltpu.VMEM((ext, model), BF16),
-         pltpu.VMEM((packed, LANES), F32), pltpu.VMEM((tp_n - 1, packed, LANES), F32),
-         pltpu.VMEM((packed, LANES), F32), pltpu.VMEM((sp_n - 1, packed, LANES), F32),
-         pltpu.VMEM((tokens, model), BF16), pltpu.VMEM((ext, model), BF16),
-         pltpu.VMEM((ctx_rows, width), BF16), pltpu.VMEM((ctx_rows, keys), BF16),
-         pltpu.VMEM((2, width, STATE), BF16), pltpu.VMEM((2 * heads, LANES), F32),
-         pltpu.VMEM((sp_n, 2, share, STATE), BF16), pltpu.VMEM((sp_n, 2 * heads, LANES), F32),
-         pltpu.VMEM((2, share, STATE), BF16),
-         dma(6), dma(tp_n), dma(tp_n), dma(tp_n), dma(tp_n), dma(sp_n), dma(sp_n), dma(2), dma(2),
-         dma(sp_n), dma(sp_n), dma(sp_n), dma(sp_n), dma(sp_n), dma(sp_n)],
+    pieces = 2 * (width // (2 * HEAD))
+    made = [
+        pltpu.VMEM((tokens, width), BF16), pltpu.VMEM((tokens, width), BF16),
+        pltpu.VMEM((tokens, keys), BF16), pltpu.VMEM((tokens, keys), BF16),
+        pltpu.VMEM((tokens, LANES), F32), pltpu.VMEM((tokens, LANES), F32),
+        pltpu.VMEM((blocks, width, 2 * STATE), F32), pltpu.VMEM((2, width, STATE), F32),
+        pltpu.VMEM((2, width, STATE), BF16), pltpu.VMEM((8, model), F32),
+    ]
+    front = [
+        pltpu.VMEM((model, width), BF16), pltpu.VMEM((model, width), BF16),
+        pltpu.VMEM((model, keys), BF16), pltpu.VMEM((model, keys), BF16),
+        pltpu.VMEM((tokens, model), BF16), pltpu.VMEM((ext, model), BF16),
+        pltpu.VMEM((packed, LANES), F32), pltpu.VMEM((tp_n - 1, packed, LANES), F32),
+        pltpu.VMEM((packed, LANES), F32), pltpu.VMEM((sp_n - 1, packed, LANES), F32),
+        pltpu.VMEM((tokens, model), BF16), pltpu.VMEM((ext, model), BF16),
+        pltpu.VMEM((ctx_rows, width), BF16), pltpu.VMEM((ctx_rows, keys), BF16),
+        pltpu.VMEM((2, width, STATE), BF16), pltpu.VMEM((2 * heads, LANES), F32),
+        pltpu.VMEM((sp_n, 2, share, STATE), BF16), pltpu.VMEM((sp_n, 2 * heads, LANES), F32),
+        pltpu.VMEM((2, share, STATE), BF16),
+        dma(6), dma(max(6, tp_n)), dma(max(6, tp_n)), dma(tp_n), dma(tp_n),
+        dma(sp_n), dma(sp_n), dma(2), dma(2),
+        dma(sp_n), dma(sp_n), dma(sp_n), dma(sp_n), dma(sp_n), dma(sp_n),
+    ]
+    assert len(front) == FRONT
+    sweep = [
+        pltpu.VMEM((2, width, STATE), BF16), pltpu.VMEM((2, width, STATE), BF16),
+        pltpu.VMEM((blocks, width, STATE), BF16), pltpu.VMEM((blocks, width, STATE), BF16),
+        pltpu.VMEM((tokens, width), F32), dma(pieces), dma(pieces),
+    ]
+    finish = [
+        pltpu.VMEM((tokens, width), BF16), pltpu.VMEM((width, model), BF16), dma(1),
+        pltpu.VMEM((tokens, model), BF16), pltpu.VMEM((2, rows // 2, model), BF16),
+        pltpu.VMEM((2, rows // 2, model), BF16), pltpu.VMEM((tp_n - 1, rows, model), BF16),
+        dma(6), dma(6),
+    ]
+    total, gate_row = call(
+        functools.partial(whole_kernel, sp_n, tp_n, heads, per_group),
+        [shape((rows, model), BF16), shape((1, model), F32)],
+        [vmem()] * 6 + [held] * 4 + [vmem()] * 7 + [held],
+        made + front + sweep + finish,
         0,
     )(act, shift_matrix, scale_matrix, gate_matrix, latent[0], context[0],
       value_proj, gate_proj, write_proj, read_proj, step_cols,
-      rates, pacing, value_taps, write_taps, read_taps)
-
-    pieces = 2 * (width // (2 * HEAD))
-    inner = call(
-        functools.partial(sweep_kernel, sp_n, heads, per_group),
-        shape((tokens, width), BF16),
-        [vmem()] * 10,
-        [pltpu.VMEM((2, width, STATE), BF16), pltpu.VMEM((2, width, STATE), BF16),
-         pltpu.VMEM((blocks, width, STATE), BF16), pltpu.VMEM((blocks, width, STATE), BF16),
-         pltpu.VMEM((tokens, width), F32), dma(pieces), dma(pieces)],
-        1,
-    )(values, gate, writes, reads, step, cumul, inc, ends, ctx, norm_gain[None])
-
-    total = call(
-        functools.partial(finish_kernel, tp_n),
-        shape((rows, model), BF16),
-        [vmem()] * 2,
-        [pltpu.VMEM((tokens, model), BF16), pltpu.VMEM((2, rows // 2, model), BF16),
-         pltpu.VMEM((2, rows // 2, model), BF16), pltpu.VMEM((tp_n - 1, rows, model), BF16),
-         dma(6), dma(6)],
-        2,
-    )(inner, out_proj)
-    updated = latent[0].astype(F32) + mod[4:5] * lax.optimization_barrier(total).astype(F32)
+      decay_rate, pacing, value_taps, write_taps, read_taps, norm_gain[None], out_proj)
+    updated = latent[0].astype(F32) + gate_row * lax.optimization_barrier(total).astype(F32)
     return updated.astype(BF16)[None]
 
 

time: 97.6 us -> 83.9 us (0.86)
  Pallas kernels: 90.4 us -> 78.4 us
    pallas_call x3 -> x1, Pallas kernels: 90.4 us -> 78.4 us  [per_device(): call(functools.partial(whole_kernel, sp_n, tp_n, heads, per_group), [shap...]
where the time goes in v3:
time: 83.9 us; the launch traced here: 83.8 us
  Pallas kernels  78.4 us (93%)
  other arithmetic  2.7 us (3%)
  local copies, waits for them, and re-layouts  2.65 us (3%)
    pallas_call x1, Pallas kernels, per_device(): call(functools.partial(whole_kernel, sp_n, tp_n, heads, per_group), [shap...  78.4 us
    broadcast_in_dim x1, other arithmetic, per_device(): return updated.astype(BF16)[None]  2 us

profile of v3, /device:TPU:0, one launch (start us, length us, event | category | flops | bytes accessed | tf_op | source)
XLA Modules:
  0.0 83.8 jit_solution(14192724308953677828)
XLA Ops:
  0.0 0.0 copy-start
  0.0 0.7 dynamic-slice_bitcast_fusion.1
  0.7 0.8 dynamic_slice.10
  1.5 0.7 multiply_convert_fusion.refs_0_
  2.2 0.0 copy-done
  2.2 0.3 copy.21
  2.5 0.9 %pad.4.refs_10_ = bf16[2048,128]{1,0:T(8,128)(2,1)} pad(bf16[2048,16]{1,0:T(8,128)(2,1)S(1)} %copy.21, bf16[]{:T(256)} %constant.36.clone.1), padding=0_0x0_112 | pad | bytes 589826 | tf_op jit(solution)/shard_map/jit(_pad)/pad | solution.py:627
  3.4 0.0 copy-start.1
  3.4 78.4 %shard_map.181 = (bf16[128,2048]{1,0:T(8,128)(2,1)}, f32[1,2048]{1,0:T(1,128)}) custom-call(bf16[48,128]{1,0:T(8,128)(2,1)} %multiply_convert_fusion.refs_0_, bf16[128,2048]{1,0:T(8,128)(2,1)} %refs_1_.1, bf16[128,2048]{1,0:T(8,128)(2,1)} %refs_2_.1, bf16[128,2048]{1,0:T(8,128)(2,1)} %refs_3_.1, bf16[128,2048]{1,0:T(8,128)(2,1)} %bitcast.11, ...), custom_call_target="tpu_custom_call" | custom-call | tf_op jit(solution)/shard_map/pallas_call | solution.py:667
  81.7 0.0 copy-done.1
  81.8 2.0 %fusion = bf16[1,128,2048]{2,1,0:T(8,128)(2,1)} fusion(bf16[128,2048]{1,0:T(8,128)(2,1)} %get-tuple-element.8, f32[2048]{0:T(1024)} %bitcast.14, bf16[1,128,2048]{2,1,0:T(8,128)(2,1)S(1)} %copy-done.1), kind=kLoop, calls=%fused_computation.1 | loop fusion | flops 1310720 | bytes 1581056 | tf_op jit(solution)/shard_map/broadcast_in_dim | solution.py:677
  (2 shorter events, 0.0 us)
Async XLA Ops:
  0.0 2.2 %copy-start = (bf16[2048,2,32]{0,2,1:T(8,128)(2,1)S(1)}, bf16[2048,2,32]{0,2,1:T(8,128)(2,1)}, u32[]{:S(2)}) copy-start(bf16[2048,2,32]{0,2,1:T(8,128)(2,1)} %param.30) | copy-start | bytes 786436
  3.4 78.4 %copy-start.1 = (bf16[1,128,2048]{2,1,0:T(8,128)(2,1)S(1)}, bf16[1,128,2048]{2,1,0:T(8,128)(2,1)}, u32[]{:S(2)}) copy-start(bf16[1,128,2048]{2,1,0:T(8,128)(2,1)} %param.19) | copy-start | bytes 1572868
